TPU v7x, 512 devices: a whole 4x4x16 slice. The times are simulated.
512 devices in a mesh: sp: 16 (over z), fs: 4 (over y), tp: 8 (over x, core).
Axes of the slice: x: 4, y: 4, z: 16, core: 2. Of those that a mesh axis runs over, the one named last changes fastest.
Arguments:
- inputs: bfloat16 [4, 4096, 4096], P('fs', 'sp', 'tp'), may hold values from -6 to 6
- norm_gain: float32 [4096], replicated, may hold values from 0.1 to 1.9
- conv_in_a: bfloat16 [4096, 1024], P(('sp', 'fs'), 'tp'), may hold values from -0.09375 to 0.09375
- conv_in_b: bfloat16 [4096, 1024], P(('sp', 'fs'), 'tp'), may hold values from -0.09375 to 0.09375
- query_w: bfloat16 [4096, 512], P(('sp', 'fs'), 'tp'), may hold values from -0.09375 to 0.09375
- key_w: bfloat16 [4096, 512], P(('sp', 'fs'), 'tp'), may hold values from -0.09375 to 0.09375
- value_w: bfloat16 [4096, 1024], P(('sp', 'fs'), 'tp'), may hold values from -0.09375 to 0.09375
- out_gate_w: bfloat16 [4096, 1024], P(('sp', 'fs'), 'tp'), may hold values from -0.09375 to 0.09375
- pointwise_w: bfloat16 [4096, 1024], P(('sp', 'fs'), 'tp'), may hold values from -0.1875 to 0.1875
- gla_out_w: bfloat16 [4096, 1024], P(('sp', 'fs'), 'tp'), may hold values from -0.1875 to 0.1875
- forget_first_factor: bfloat16 [4096, 64], replicated, may hold values from -0.09375 to 0.09375
- decay_w: bfloat16 [64, 512], replicated, may hold values from -0.75 to 0.75
- decay_bias: float32 [512], replicated, as said below
- decay_extra: float32 [4, 4096, 512], P('fs', 'sp', 'tp'), may hold values from -2.2 to 0, as said below
- conv_kernel: float32 [31, 1024], replicated, may hold values from -7 to 7
- conv_gain: float32 [1024], replicated, may hold values from 0.1 to 1.9
- head_gain: float32 [64], replicated, may hold values from 0.1 to 1.9
Outputs:
- mixed: bfloat16 [4, 4096, 4096], P('fs', 'sp', 'tp')
Inputs may be any that keep to these rules, and one draw needn't show every extreme that they name: decay_bias is positive. decay_extra is never positive.
All inputs are finite; a program needn't handle non-finite values.
Results may differ from a plain program's by a relative error of at most 0.015.
Values may be sent and summed in bfloat16 or wider, within the bound.
A program may use at most 128 MiB of HBM per device.

v0:
```python
import jax
import jax.numpy as jnp
from jax import lax
from jax.sharding import PartitionSpec as P

DK = 32
DV = 64
BLOCK = 64


def side_by_side(arrays, axis, dim, along):
    ends, at = ([], 0)
    for a in arrays[:-1]:
        at += a.shape[along]
        ends.append(at)
    both = jnp.concatenate(arrays, axis=along)
    return tuple(jnp.split(lax.all_gather(both, axis, axis=dim, tiled=True), ends, axis=along))


def from_everyone(value, axis):
    length = lax.axis_size(axis)
    return lax.all_to_all(
        jnp.broadcast_to(value[None], (length, *value.shape)), axis, 0, 0, tiled=True
    )


def in_order(tiles, dim):
    lengths = list(tiles.shape[1:])
    lengths[dim] *= tiles.shape[0]
    return jnp.moveaxis(tiles, 0, dim).reshape(lengths)


def gathered_copies(value, axis, dim):
    tiles = from_everyone(value, axis)
    return in_order(tiles, dim)


def from_behind(value, axis, by):
    length = lax.axis_size(axis)
    pairs = [(i, i + by) for i in range(length) if 0 <= i + by < length]
    return lax.ppermute(value, axis, pairs)


def over_copies(value, axis):
    everything = from_everyone(value, axis)
    return jnp.sum(everything, axis=0)


def in_one(arrays, axis):
    vector, at, outs = (jnp.concatenate([a.reshape(-1) for a in arrays]), 0, [])
    subtotal = over_copies(vector, axis)
    for a in arrays:
        outs.append(subtotal[at : at + a.size].reshape(a.shape))
        at += a.size
    return tuple(outs)


def in_blocks(value, dim, length):
    lengths = value.shape
    tiles = value.reshape(*lengths[:dim], length, lengths[dim] // length, *lengths[dim + 1 :])
    return jnp.moveaxis(tiles, dim, 0)


def sum_at_owner(value, axis, dim):
    length = lax.axis_size(axis)
    tiles = lax.all_to_all(in_blocks(value, dim, length), axis, 0, 0, tiled=True)
    return jnp.sum(tiles.astype(jnp.float32), axis=0)


def shards(
    inputs,
    norm_gain,
    conv_in_a,
    conv_in_b,
    query_w,
    key_w,
    value_w,
    out_gate_w,
    pointwise_w,
    gla_out_w,
    forget_first_factor,
    decay_w,
    decay_bias,
    decay_extra,
    conv_kernel,
    conv_gain,
    head_gain,
):
    nearer = side_by_side(
        (conv_in_a, conv_in_b, query_w, key_w, value_w, out_gate_w, pointwise_w, gla_out_w),
        "fs",
        0,
        1,
    )
    collected = side_by_side(
        (nearer[0], nearer[1], nearer[2], nearer[3], nearer[4], nearer[5], nearer[6], nearer[7]),
        "sp",
        0,
        1,
    )
    (
        conv_a_full,
        conv_b_full,
        query_full,
        key_full,
        value_full,
        gate_full,
        pointwise_full,
        gla_out_full,
    ) = collected
    tok_rows = inputs[0]
    token_count = tok_rows.shape[0]
    in_weights = (
        conv_a_full,
        conv_b_full,
        query_full,
        key_full,
        value_full,
        gate_full,
        forget_first_factor,
    )
    segment_values = gathered_copies(tok_rows, "tp", 1).astype(jnp.float32)
    scaled = (segment_values * norm_gain).astype(jnp.bfloat16)
    sums = tuple(
        (jnp.dot(scaled, weight, preferred_element_type=jnp.float32) for weight in in_weights)
    )
    sums, squares = (sums, jnp.sum(segment_values * segment_values, axis=1))
    row_scale = lax.rsqrt(squares / norm_gain.shape[0] + 1e-06)[:, None]
    conv_a, conv_b, queries, keys, values, out_gate, low_rank = [
        (running * row_scale).astype(jnp.bfloat16) for running in sums
    ]
    gated = (conv_a.astype(jnp.float32) * jax.nn.sigmoid(conv_b.astype(jnp.float32))).astype(
        jnp.bfloat16
    )
    reach = conv_kernel.shape[0] - 1
    earlier = from_behind(gated[token_count - reach :], "sp", 1)
    extended = jnp.concatenate([earlier, gated], axis=0).astype(jnp.float32)
    tp_index = lax.axis_index("tp")
    channels = gated.shape[1]
    kernel = lax.dynamic_slice_in_dim(conv_kernel, tp_index * channels, channels, 1)
    convolved = jnp.zeros((token_count, channels), jnp.float32)
    for offset in range(reach + 1):
        convolved = convolved + kernel[offset] * extended[offset : offset + token_count]
    channel_sum, channel_squares = in_one(
        (jnp.sum(convolved, axis=1), jnp.sum(convolved * convolved, axis=1)), "tp"
    )
    total_channels = conv_gain.shape[0]
    average = channel_sum / total_channels
    spread_squared_mean = channel_squares / total_channels - average * average
    gain_part = lax.dynamic_slice_in_dim(conv_gain, tp_index * channels, channels)
    normed = (
        (convolved - average[:, None]) * lax.rsqrt(spread_squared_mean + 1e-05)[:, None] * gain_part
    )
    conv_act = jax.nn.silu(normed).astype(jnp.bfloat16)
    key_width = keys.shape[1]
    head_count = key_width // DK
    decay_part = lax.dynamic_slice_in_dim(decay_w, tp_index * key_width, key_width, 1)
    bias_part = lax.dynamic_slice_in_dim(decay_bias, tp_index * key_width, key_width)
    pre_decay = jnp.dot(low_rank, decay_part, preferred_element_type=jnp.float32) + bias_part
    log_decay = jax.nn.log_sigmoid(pre_decay) / 16.0 + decay_extra[0]
    block_count = token_count // BLOCK
    highest = lax.Precision.HIGHEST

    def split_blocks(array_operand, width):
        return array_operand.reshape(block_count, BLOCK, head_count, width).transpose(0, 2, 1, 3)

    q_blocks = split_blocks(queries.astype(jnp.float32), DK) * DK ** (-0.5)
    k_blocks = split_blocks(keys.astype(jnp.float32), DK)
    v_blocks = split_blocks(values.astype(jnp.float32), DV)
    prefix_running_sum = jnp.cumsum(split_blocks(log_decay, DK), axis=2)
    causal = jnp.tril(jnp.ones((BLOCK, BLOCK), dtype=bool))
    spread = prefix_running_sum[:, :, :, None, :] - prefix_running_sum[:, :, None, :, :]
    weights_in = jnp.exp(jnp.where(causal[:, :, None], spread, -jnp.inf))
    scores = jnp.einsum("nhid,nhjd,nhijd->nhij", q_blocks, k_blocks, weights_in, precision=highest)
    inner = jnp.einsum("nhij,nhjv->nhiv", scores, v_blocks, precision=highest)
    block_total = prefix_running_sum[:, :, -1]
    block_state = jnp.einsum(
        "nhjd,nhjv->nhdv",
        k_blocks * jnp.exp(block_total[:, :, None] - prefix_running_sum),
        v_blocks,
        precision=highest,
    )

    def advance(state, block_pair):
        decay_row, added_share_term = block_pair
        return (jnp.exp(decay_row)[..., None] * state + added_share_term, state)

    local_final, local_entering = lax.scan(
        advance, jnp.zeros((head_count, DK, DV), jnp.float32), (block_total, block_state)
    )
    device_total = jnp.sum(block_total, axis=0)
    totals = lax.all_gather(device_total[None], "sp", axis=0, tiled=True)
    running_totals = jnp.cumsum(totals, axis=0)
    sp_index = lax.axis_index("sp")
    before = lax.dynamic_index_in_dim(
        running_totals, sp_index, 0, False
    ) - lax.dynamic_index_in_dim(totals, sp_index, 0, False)
    piece = lax.all_gather(local_final[None], "sp", axis=0, tiled=True)
    number = piece.shape[0]
    anchor = jnp.arange(number, dtype=jnp.int32)
    exponent = jnp.where(
        (anchor < sp_index)[:, None, None], before[None] - running_totals, -jnp.inf
    )
    entering = jnp.einsum("nhd,nhdv->hdv", jnp.exp(exponent), piece, precision=highest)
    passed = jnp.exp(jnp.cumsum(block_total, axis=0) - block_total)
    entering_blocks = passed[..., None] * entering[None] + local_entering
    outer = jnp.einsum(
        "nhid,nhdv->nhiv",
        q_blocks * jnp.exp(prefix_running_sum),
        entering_blocks,
        precision=highest,
    )
    head_output = inner + outer
    normed_heads = (
        head_output
        * lax.rsqrt(jnp.mean(head_output * head_output, axis=-1, keepdims=True) + 1e-06)
        * head_gain
    )
    gla_rows = normed_heads.transpose(0, 2, 1, 3).reshape(token_count, head_count * DV)
    gla_act = (gla_rows * jax.nn.silu(out_gate.astype(jnp.float32))).astype(jnp.bfloat16)
    contract = (((1,), (1,)), ((), ()))
    conv_term = lax.dot_general(
        pointwise_full, conv_act, contract, preferred_element_type=jnp.float32
    )
    summed = sum_at_owner(
        (
            conv_term
            + lax.dot_general(gla_out_full, gla_act, contract, preferred_element_type=jnp.float32)
        ).astype(jnp.bfloat16),
        "tp",
        0,
    )
    return (tok_rows.astype(jnp.float32) + summed.T).astype(jnp.bfloat16)[None]


def solution(mesh):
    return jax.shard_map(
        shards,
        mesh=mesh,
        in_specs=(
            P("fs", "sp", "tp"),
            P(),
            P(("sp", "fs"), "tp"),
            P(("sp", "fs"), "tp"),
            P(("sp", "fs"), "tp"),
            P(("sp", "fs"), "tp"),
            P(("sp", "fs"), "tp"),
            P(("sp", "fs"), "tp"),
            P(("sp", "fs"), "tp"),
            P(("sp", "fs"), "tp"),
            P(),
            P(),
            P(),
            P("fs", "sp", "tp"),
            P(),
            P(),
            P(),
        ),
        out_specs=P("fs", "sp", "tp"),
        check_vma=False,
    )
```

profile of v0, /device:TPU:1, one launch (start us, length us, event | category | flops | bytes accessed | tf_op | source)
XLA Modules:
  0.0 245.8 jit_solution(409942196637541957)
XLA Ops:
  6.5 1.0 concatenate.11
  7.5 12.3 %all_gather.12 = bf16[256,896]{1,0:T(8,128)(2,1)} all-gather(bf16[64,896]{1,0:T(8,128)(2,1)S(1)} %concatenate.11), channel_id=1, replica_groups=mesh['sp'=16,'fs'=4,'tp'=8] {'fs'}, dimensions={0}, use_global_device_ids=true | all-gather | bytes 573440 | tf_op jit(solution)/shard_map/all_gather | solution.py:17
  19.8 1.1 copy.64
  20.9 1.5 broadcast_in_dim.45
  22.4 11.6 %all-to-all-start = ((bf16[8,256,512]{1,2,0:T(8,128)(2,1)}), bf16[8,256,512]{1,2,0:T(8,128)(2,1)S(1)}, u32[]{:S(2)}, u32[]{:S(2)}) async-start(bf16[8,256,512]{1,2,0:T(8,128)(2,1)} %broadcast_in_dim.45), calls=%async_computation | async-start | bytes 4194304 | tf_op jit(solution)/shard_map/all_to_all | solution.py:22
  34.0 0.8 dynamic_slice.30
  34.8 1.3 dynamic_slice.28
  36.1 1.7 dynamic-slice_bitcast_fusion.29
  37.8 1.9 fusion.98
  39.7 20.6 %all-to-all-done = bf16[8,256,512]{1,2,0:T(8,128)(2,1)S(1)} async-done(((bf16[8,256,512]{1,2,0:T(8,128)(2,1)}), bf16[8,256,512]{1,2,0:T(8,128)(2,1)S(1)}, u32[]{:S(2)}, u32[]{:S(2)}) %all-to-all-start) | async-done | bytes 2097184 | tf_op jit(solution)/shard_map/all_to_all | solution.py:22
  60.9 1.8 fusion.2
  62.6 2.2 fusion.86
  65.5 28.2 %all-gather.2 = f32[16,2,32]{2,1,0:T(2,128)S(1)} all-gather(f32[1,2,32]{2,1,0:T(2,128)S(1)} %bitcast.160), channel_id=2, replica_groups=mesh['sp'=16,'fs'=4,'tp'=8] {'sp'}, dimensions={0}, use_global_device_ids=true | all-gather | bytes 4352 | tf_op jit(solution)/shard_map/all_gather | solution.py:192
  94.0 4.6 %select_exponential_fusion = f32[4,2,64,64,32]{3,4,2,1,0:T(8,128)} fusion(f32[4,2,64,32]{2,3,1,0:T(8,128)S(1)} %copy.67, f32[4,2,64,32]{3,2,1,0:T(8,128)S(1)} %reduce_window_sum.35, pred[64,64]{1,0:T(8,128)(4,1)S(1)} %iota_compare_fusion), kind=kLoop, calls=%fused_computation.5 | loop fusion | flops 2097152 | bytes 4329472 | tf_op jit(solution)/shard_map/exp | solution.py:173
  98.5 11.0 %copy.82 = f32[4,2,64,64,32]{2,3,4,1,0:T(8,128)} copy(f32[4,2,64,64,32]{3,4,2,1,0:T(8,128)} %select_exponential_fusion) | data formatting | bytes 8388608
  109.6 12.5 %all-gather.5.cloned.1.call-done = bf16[4096,896]{1,0:T(8,128)(2,1)} async-done(((bf16[256,896]{1,0:T(8,128)(2,1)}), bf16[4096,896]{1,0:T(8,128)(2,1)}) %all-gather.5.cloned.1.call-update) | async-done | bytes 7340048 | tf_op jit(solution)/shard_map/all_gather | solution.py:17
  122.1 2.2 fusion.18
  124.4 0.8 copy.73
  125.3 2.0 fusion.13
  127.4 2.0 fusion.38
  129.4 5.8 %while.13 = (s32[]{:T(128)}, f32[2,32,64]{2,1,0:T(8,128)S(1)}, f32[4,2,32,64]{3,2,1,0:T(8,128)}, f32[4,2,32]{2,1,0:T(2,128)S(1)}, f32[4,2,32,64]{3,2,1,0:T(8,128)}, /*index=5*/s32[]{:T(128)}, s32[]{:T(128)}) while((s32[]{:T(128)}, f32[2,32,64]{2,1,0:T(8,128)S(1)}, f32[4,2,32,64]{3,2,1,0:T(8,128)}, f32[4,2,32]{2,1,0:T(2,128)S(1)}, ...), condition=%wide.region_9.10_spmd.clone, body=%wide.region_8.9_spmd.clone.sunk | while | flops 16387 | bytes 99680 | solution.py:188
  129.4 0.6 bitcast_dynamic-update-slice_fusion.2
  130.0 0.8 bitcast_add_fusion.3
  130.8 0.6 bitcast_dynamic-update-slice_fusion.2
  131.4 0.8 bitcast_add_fusion.3
  132.3 0.6 bitcast_dynamic-update-slice_fusion.2
  132.9 0.8 bitcast_add_fusion.3
  133.7 0.6 bitcast_dynamic-update-slice_fusion.2
  134.3 0.8 bitcast_add_fusion.3
  135.2 25.9 %all-gather.1 = f32[32,32,64]{2,1,0:T(8,128)} all-gather(f32[2,32,64]{2,1,0:T(8,128)S(1)} %get-tuple-element.33), channel_id=3, replica_groups=mesh['sp'=16,'fs'=4,'tp'=8] {'sp'}, dimensions={0}, use_global_device_ids=true | all-gather | bytes 278528 | tf_op jit(solution)/shard_map/all_gather | solution.py:198
  161.1 0.7 copy.68
  161.7 1.8 fusion.21
  163.6 0.8 copy.72
  164.5 5.3 %fusion = f32[4,2,64,64]{2,3,1,0:T(8,128)S(1)} fusion(f32[4,2,64,64,32]{2,3,4,1,0:T(8,128)} %copy.82, f32[4,2,32,64]{3,2,1,0:T(8,128)S(1)} %copy.69, f32[4,2,32,64]{3,2,1,0:T(8,128)} %copy.68), kind=kLoop, calls=%fused_computation.4 | loop fusion | flops 3112960 | bytes 4456448 | tf_op jit(solution)/shard_map/nhid,nhjd,nhijd->nhij/dot_general | solution.py:174
  170.4 2.0 fusion.12
  172.4 2.0 fusion.6
  174.4 2.2 collective-permute-start
  176.7 0.9 fusion.34
  177.6 0.8 multiply_reduce_fusion.1
  178.7 1.2 fusion.101
  179.8 0.6 broadcast_in_dim.46
  180.4 12.4 %all-to-all-start.1 = ((f32[8,1,512]{2,1,0:T(1,128)}), f32[8,1,512]{2,1,0:T(1,128)S(1)}, u32[]{:S(2)}, u32[]{:S(2)}) async-start(f32[8,1,512]{2,1,0:T(1,128)} %broadcast_in_dim.46), calls=%async_computation.1 | async-start | bytes 32768 | tf_op jit(solution)/shard_map/all_to_all | solution.py:22
  192.9 0.7 fusion.37
  194.0 3.6 %all-to-all-done.1 = f32[8,1,512]{2,1,0:T(1,128)S(1)} async-done(((f32[8,1,512]{2,1,0:T(1,128)}), f32[8,1,512]{2,1,0:T(1,128)S(1)}, u32[]{:S(2)}, u32[]{:S(2)}) %all-to-all-start.1) | async-done | bytes 16416 | tf_op jit(solution)/shard_map/all_to_all | solution.py:22
  197.6 4.1 %fusion.31 = f32[4096,256]{1,0:T(8,128)} fusion(bf16[4096,896]{1,0:T(8,128)(2,1)} %all-gather.5.cloned.1.call-done, f32[256,128]{1,0:T(8,128)} %get-tuple-element.65, f32[128]{0:T(128)} %dynamic_slice.28, f32[256]{0:T(256)S(1)} %get-tuple-element.100, f32[256]{0:T(256)S(1)} %get-tuple-element.99), kind=kOutput, calls=%fused_computation.50 | convolution fusion | flops 268697600 | bytes 5376512 | tf_op jit(solution)/shard_map/dot_general | solution.py:222
  201.7 5.7 %fusion.1 = bf16[4096,256]{1,0:T(8,128)(2,1)} fusion(f32[4096,256]{1,0:T(8,128)} %fusion.31, bf16[4096,896]{1,0:T(8,128)(2,1)} %all-gather.5.cloned.1.call-done, f32[256,128]{1,0:T(8,128)S(1)} %reshape.78, bf16[256,4096]{0,1:T(8,128)(2,1)S(1)} %copy-done.1, f32[256]{0:T(256)S(1)} %add_rsqrt_fusion.1), kind=kOutput, calls=%fused_computation.7 | convolution fusion | flops 539262976 | bytes 10617856 | tf_op jit(solution)/shard_map/dot_general | solution.py:228
  207.3 30.4 %all_to_all.16 = bf16[8,512,256]{2,1,0:T(8,128)(2,1)S(1)} all-to-all(bf16[8,512,256]{2,1,0:T(8,128)(2,1)} %bitcast.150), channel_id=1, replica_groups=mesh['sp'=16,'fs'=4,'tp'=8] {'tp'}, dimensions={0} | all-to-all | bytes 4194304 | tf_op jit(solution)/shard_map/all_to_all | solution.py:66
  238.1 0.8 copy.77
  (112 shorter events, 3.1 us)
Async XLA Ops:
  6.5 56.1 %copy-start = (bf16[4096,64]{0,1:T(8,128)(2,1)S(1)}, bf16[4096,64]{0,1:T(8,128)(2,1)}, u32[]{:S(2)}) copy-start(bf16[4096,64]{0,1:T(8,128)(2,1)} %param.29) | copy-start | bytes 1572868
  6.5 115.5 %all-gather.5.cloned.1.call-start = ((), (), s32[]{:S(2)}) async-start(), calls=%async_computation.3 | async-start | bytes 7798784 | tf_op jit(solution)/shard_map/all_gather | solution.py:17
  20.9 39.9 %copy-start.6 = (f32[4096]{0:T(1024)S(1)}, f32[4096]{0:T(1024)}, u32[]{:S(2)}) copy-start(f32[4096]{0:T(1024)} %param.20) | copy-start | bytes 49156
  22.4 37.8 %all-to-all-start = ((bf16[8,256,512]{1,2,0:T(8,128)(2,1)}), bf16[8,256,512]{1,2,0:T(8,128)(2,1)S(1)}, u32[]{:S(2)}, u32[]{:S(2)}) async-start(bf16[8,256,512]{1,2,0:T(8,128)(2,1)} %broadcast_in_dim.45), calls=%async_computation | async-start | bytes 4194304 | tf_op jit(solution)/shard_map/all_to_all | solution.py:22
  34.0 28.6 %copy-start.5 = (f32[1,256,64]{1,2,0:T(8,128)S(1)}, f32[1,256,64]{1,2,0:T(8,128)}, u32[]{:S(2)}) copy-start(f32[1,256,64]{1,2,0:T(8,128)} %param.32) | copy-start | bytes 196612
  98.5 23.5 %copy-start.1 = (bf16[256,4096]{0,1:T(8,128)(2,1)S(1)}, bf16[256,4096]{0,1:T(8,128)(2,1)}, u32[]{:S(2)}) copy-start(bf16[256,4096]{0,1:T(8,128)(2,1)} %fusion.2) | copy-start | bytes 6291460
  169.8 6.9 %copy-start.2 = (f32[32,32,64]{2,1,0:T(8,128)S(1)}, f32[32,32,64]{2,1,0:T(8,128)}, u32[]{:S(2)}) copy-start(f32[32,32,64]{2,1,0:T(8,128)} %all-gather.1) | copy-start | bytes 786436
  170.1 7.4 %copy-start.3 = (f32[4,64,2,32]{3,1,2,0:T(8,128)S(1)}, f32[4,64,2,32]{3,1,2,0:T(8,128)}, u32[]{:S(2)}) copy-start(f32[4,64,2,32]{3,1,2,0:T(8,128)} %copy.72) | copy-start | bytes 196612
  170.1 7.4 %copy-start.4 = (f32[4,2,32,64]{3,2,1,0:T(8,128)S(1)}, f32[4,2,32,64]{3,2,1,0:T(8,128)}, u32[]{:S(2)}) copy-start(f32[4,2,32,64]{3,2,1,0:T(8,128)} %get-tuple-element.34) | copy-start | bytes 196612
  170.1 8.2 %copy-start.7 = (f32[128]{0:T(128)S(1)}, f32[128]{0:T(128)}, u32[]{:S(2)}) copy-start(f32[128]{0:T(128)} %get-tuple-element.69) | copy-start | bytes 1540
  170.1 8.2 %copy-start.8 = (f32[128]{0:T(128)S(1)}, f32[128]{0:T(128)}, u32[]{:S(2)}) copy-start(f32[128]{0:T(128)} %get-tuple-element.70) | copy-start | bytes 1540
  170.1 8.2 %copy-start.9 = (f32[128]{0:T(128)S(1)}, f32[128]{0:T(128)}, u32[]{:S(2)}) copy-start(f32[128]{0:T(128)} %get-tuple-element.71) | copy-start | bytes 1540
  170.2 8.2 %copy-start.10 = (f32[128]{0:T(128)S(1)}, f32[128]{0:T(128)}, u32[]{:S(2)}) copy-start(f32[128]{0:T(128)} %get-tuple-element.72) | copy-start | bytes 1540
  170.2 8.2 %copy-start.11 = (f32[128]{0:T(128)S(1)}, f32[128]{0:T(128)}, u32[]{:S(2)}) copy-start(f32[128]{0:T(128)} %get-tuple-element.73) | copy-start | bytes 1540
  170.2 8.2 %copy-start.12 = (f32[128]{0:T(128)S(1)}, f32[128]{0:T(128)}, u32[]{:S(2)}) copy-start(f32[128]{0:T(128)} %get-tuple-element.74) | copy-start | bytes 1540
  170.2 8.2 %copy-start.13 = (f32[128]{0:T(128)S(1)}, f32[128]{0:T(128)}, u32[]{:S(2)}) copy-start(f32[128]{0:T(128)} %get-tuple-element.75) | copy-start | bytes 1540
  170.2 8.2 %copy-start.14 = (f32[128]{0:T(128)S(1)}, f32[128]{0:T(128)}, u32[]{:S(2)}) copy-start(f32[128]{0:T(128)} %get-tuple-element.76) | copy-start | bytes 1540
  170.2 8.2 %copy-start.15 = (f32[128]{0:T(128)S(1)}, f32[128]{0:T(128)}, u32[]{:S(2)}) copy-start(f32[128]{0:T(128)} %get-tuple-element.77) | copy-start | bytes 1540
  170.2 8.2 %copy-start.16 = (f32[128]{0:T(128)S(1)}, f32[128]{0:T(128)}, u32[]{:S(2)}) copy-start(f32[128]{0:T(128)} %get-tuple-element.78) | copy-start | bytes 1540
  170.2 8.2 %copy-start.17 = (f32[128]{0:T(128)S(1)}, f32[128]{0:T(128)}, u32[]{:S(2)}) copy-start(f32[128]{0:T(128)} %get-tuple-element.79) | copy-start | bytes 1540
  170.2 8.2 %copy-start.18 = (f32[128]{0:T(128)S(1)}, f32[128]{0:T(128)}, u32[]{:S(2)}) copy-start(f32[128]{0:T(128)} %get-tuple-element.80) | copy-start | bytes 1540
  170.2 8.2 %copy-start.19 = (f32[128]{0:T(128)S(1)}, f32[128]{0:T(128)}, u32[]{:S(2)}) copy-start(f32[128]{0:T(128)} %get-tuple-element.81) | copy-start | bytes 1540
  170.3 8.2 %copy-start.20 = (f32[128]{0:T(128)S(1)}, f32[128]{0:T(128)}, u32[]{:S(2)}) copy-start(f32[128]{0:T(128)} %get-tuple-element.82) | copy-start | bytes 1540
  170.3 8.2 %copy-start.21 = (f32[128]{0:T(128)S(1)}, f32[128]{0:T(128)}, u32[]{:S(2)}) copy-start(f32[128]{0:T(128)} %get-tuple-element.83) | copy-start | bytes 1540
  170.3 8.2 %copy-start.22 = (f32[128]{0:T(128)S(1)}, f32[128]{0:T(128)}, u32[]{:S(2)}) copy-start(f32[128]{0:T(128)} %get-tuple-element.84) | copy-start | bytes 1540
  170.3 8.2 %copy-start.23 = (f32[128]{0:T(128)S(1)}, f32[128]{0:T(128)}, u32[]{:S(2)}) copy-start(f32[128]{0:T(128)} %get-tuple-element.85) | copy-start | bytes 1540
  170.3 8.2 %copy-start.24 = (f32[128]{0:T(128)S(1)}, f32[128]{0:T(128)}, u32[]{:S(2)}) copy-start(f32[128]{0:T(128)} %get-tuple-element.86) | copy-start | bytes 1540
  170.3 8.2 %copy-start.25 = (f32[128]{0:T(128)S(1)}, f32[128]{0:T(128)}, u32[]{:S(2)}) copy-start(f32[128]{0:T(128)} %get-tuple-element.87) | copy-start | bytes 1540
  170.3 8.2 %copy-start.26 = (f32[128]{0:T(128)S(1)}, f32[128]{0:T(128)}, u32[]{:S(2)}) copy-start(f32[128]{0:T(128)} %get-tuple-element.88) | copy-start | bytes 1540
  170.3 8.2 %copy-start.27 = (f32[128]{0:T(128)S(1)}, f32[128]{0:T(128)}, u32[]{:S(2)}) copy-start(f32[128]{0:T(128)} %get-tuple-element.89) | copy-start | bytes 1540
  170.3 8.2 %copy-start.28 = (f32[128]{0:T(128)S(1)}, f32[128]{0:T(128)}, u32[]{:S(2)}) copy-start(f32[128]{0:T(128)} %get-tuple-element.90) | copy-start | bytes 1540
  170.3 8.2 %copy-start.29 = (f32[128]{0:T(128)S(1)}, f32[128]{0:T(128)}, u32[]{:S(2)}) copy-start(f32[128]{0:T(128)} %get-tuple-element.91) | copy-start | bytes 1540
  170.4 8.2 %copy-start.30 = (f32[128]{0:T(128)S(1)}, f32[128]{0:T(128)}, u32[]{:S(2)}) copy-start(f32[128]{0:T(128)} %get-tuple-element.92) | copy-start | bytes 1540
  170.4 8.2 %copy-start.31 = (f32[128]{0:T(128)S(1)}, f32[128]{0:T(128)}, u32[]{:S(2)}) copy-start(f32[128]{0:T(128)} %get-tuple-element.93) | copy-start | bytes 1540
  170.4 8.2 %copy-start.32 = (f32[128]{0:T(128)S(1)}, f32[128]{0:T(128)}, u32[]{:S(2)}) copy-start(f32[128]{0:T(128)} %get-tuple-element.94) | copy-start | bytes 1540
  170.4 8.2 %copy-start.33 = (f32[128]{0:T(128)S(1)}, f32[128]{0:T(128)}, u32[]{:S(2)}) copy-start(f32[128]{0:T(128)} %get-tuple-element.95) | copy-start | bytes 1540
  170.4 8.2 %copy-start.34 = (f32[128]{0:T(128)S(1)}, f32[128]{0:T(128)}, u32[]{:S(2)}) copy-start(f32[128]{0:T(128)} %get-tuple-element.96) | copy-start | bytes 1540
  170.4 8.2 %copy-start.35 = (f32[128]{0:T(128)S(1)}, f32[128]{0:T(128)}, u32[]{:S(2)}) copy-start(f32[128]{0:T(128)} %get-tuple-element.97) | copy-start | bytes 1540
  170.4 8.2 %copy-start.36 = (f32[128]{0:T(128)S(1)}, f32[128]{0:T(128)}, u32[]{:S(2)}) copy-start(f32[128]{0:T(128)} %get-tuple-element.98) | copy-start | bytes 1540
  174.4 3.9 %collective-permute-start = (bf16[30,128]{1,0:T(8,128)(2,1)S(1)}, bf16[30,128]{1,0:T(8,128)(2,1)S(1)}, u32[]{:S(2)}, u32[]{:S(2)}) collective-permute-start(bf16[30,128]{1,0:T(8,128)(2,1)S(1)} %slice.265), channel_id=1, source_target_pairs={{0,32},{32,64},{64,96},{96,128},{128,160},{160,192},{192,224},{224... | collective-permute-start | bytes 23048 | tf_op jit(solution)/shard_map/ppermute | solution.py:41
  180.4 17.1 %all-to-all-start.1 = ((f32[8,1,512]{2,1,0:T(1,128)}), f32[8,1,512]{2,1,0:T(1,128)S(1)}, u32[]{:S(2)}, u32[]{:S(2)}) async-start(f32[8,1,512]{2,1,0:T(1,128)} %broadcast_in_dim.46), calls=%async_computation.1 | async-start | bytes 32768 | tf_op jit(solution)/shard_map/all_to_all | solution.py:22
Sparse Core Ops, SparseCore 0:
  20.0 102.0 all-gather.4
where the time goes:
time: 247 us; the launch traced here: 246 us
  blocking collectives  96.8 us (39%)
  waiting for transfers between devices  36.6 us (15%)
  starting transfers between devices  26.3 us (11%)
  matrix products  25.9 us (10%)
  local copies, waits for them, and re-layouts  25.3 us (10%)
  other arithmetic  20.7 us (8%)
  between operations  14.1 us (6%)
    all_to_all x1, blocking collectives, sum_at_owner(): lax.all_to_all(in_blocks(value, dim, length), axis, 0, 0, tiled=True)  30.4 us
    all_gather x1, blocking collectives, shards(): totals = lax.all_gather(device_total[None], 'sp', axis=0, tiled=True)  28.2 us
    all_gather x1, blocking collectives, shards(): piece = lax.all_gather(local_final[None], 'sp', axis=0, tiled=True)  25.9 us
    all_to_all x2, waiting for transfers between devices, from_everyone(): lax.all_to_all(jnp.broadcast_to(value[None], (length, *value.shape)), axi...  24.1 us
    all_to_all x2, starting transfers between devices, from_everyone(): lax.all_to_all(jnp.broadcast_to(value[None], (length, *value.shape)), axi...  24 us
    all_gather x1, waiting for transfers between devices, side_by_side(): lax.all_gather(both, axis, axis=dim, tiled=True)  12.5 us
    all_gather x1, blocking collectives, side_by_side(): lax.all_gather(both, axis, axis=dim, tiled=True)  12.3 us
    unnamed x76, local copies, waits for them, and re-layouts  12.3 us
  transfers between devices with their start and end apart: 4, of which 3 were waited for; matrix products, arithmetic and copies ran while one was open for 13% of the time, Pallas kernels for 0%

commit v1 on v0

v1 whole, which is shorter than its diff:
```python
import functools

import jax
import jax.numpy as jnp
from jax import lax
from jax.experimental import pallas as pl
from jax.experimental.pallas import tpu as pltpu
from jax.sharding import PartitionSpec as P

MESH = pl.DeviceIdType.MESH
F32 = jnp.float32
BF16 = jnp.bfloat16
HIGHEST = lax.Precision.HIGHEST
NZ = 16
TOK = 256
NT = (((1,), (1,)), ((), ()))
TN = (((0,), (0,)), ((), ()))


def remote(src, dst, send, recv, device):
    return pltpu.make_async_remote_copy(
        src_ref=src,
        dst_ref=dst,
        send_sem=send,
        recv_sem=recv,
        device_id=device,
        device_id_type=MESH,
    )


def wrap(value, size):
    return lax.rem(value + size, size)


def rows(start, size):
    return pl.ds(pl.multiple_of(start, size), size)


def iota(shape, dim):
    return lax.broadcasted_iota(jnp.int32, shape, dim)


def sigmoid(value):
    return 1.0 / (1.0 + jnp.exp(-value))


def roll64(value):
    return pltpu.roll(value, 64, 1)


def body(
    xin,
    wsrc,
    owsrc,
    exsrc,
    dwt,
    bias,
    taps,
    cgain,
    hgain,
    out,
    xg,
    w,
    ow,
    acc_own,
    acc_send,
    acc_recv,
    mats,
    xors,
    scores,
    ext,
    exb,
    stats,
    tot_me,
    tots,
    st_me,
    sts,
    act_me,
    acts,
    po_send,
    po_recv,
    x_send1,
    x_send2,
    x_recv,
    wy_send,
    wy_recv,
    wz_send,
    wz_recv,
    ox_send,
    ox_recv,
    oz_send,
    oz_recv,
    oy_send,
    oy_recv,
    ex_send,
    ex_recv,
    d2d_send,
    d2d_recv,
    halo_send,
    halo_recv,
    stat_send,
    stat_recv,
    tot_send,
    tot_recv,
    st_send,
    st_recv,
    act_send,
    act_recv,
):
    z = lax.axis_index("sp")
    y = lax.axis_index("fs")
    t = lax.axis_index("tp")
    x = lax.div(t, 2)
    c = t - 2 * x
    y_half = lax.div(y, 2)
    y_low = y - 2 * y_half
    z_class = lax.rem(lax.div(z, 2), 2)
    partner = (z, y, 2 * x + 1 - c)

    def at(xx, yy, zz, cc):
        return (zz, yy, 2 * xx + cc)

    barrier = pltpu.get_barrier_semaphore()

    def greet_plane(k, carry):
        flat = lax.rem(y * 8 + t + k, 32)
        yy = lax.div(flat, 8)
        pl.semaphore_signal(
            barrier, inc=1, device_id=(z, yy, flat - 8 * yy), device_id_type=MESH
        )
        return carry

    lax.fori_loop(1, 32, greet_plane, 0)

    def greet_line(k, carry):
        pl.semaphore_signal(
            barrier, inc=1, device_id=(lax.rem(z + k, NZ), y, t), device_id_type=MESH
        )
        return carry

    lax.fori_loop(1, NZ, greet_line, 0)

    own_rows = y * TOK
    own_cols = pl.ds(pl.multiple_of(x * 512, 512), 512)
    xg[rows(own_rows, TOK), own_cols] = xin[...]
    pl.semaphore_wait(barrier, 31 + NZ - 1)

    finish = []

    def start(copy, cond=None):
        if cond is None:
            copy.start()
        else:
            pl.when(cond)(copy.start)
        finish.append((copy, cond))

    def w_at(zz, yy):
        at_row = lax.div(zz, 4) * 512 + lax.rem(zz, 2) * 256 + yy * 64
        return w.at[rows(at_row, 64), :]

    for j in range(2):
        mine = jnp.logical_and(2 * c + j == y, z_class == c)
        start(
            remote(
                wsrc.at[j],
                w_at(z, y),
                wy_send.at[j],
                wy_recv.at[y],
                at(x, 2 * c + j, z, z_class),
            ),
            jnp.logical_not(mine),
        )

        @pl.when(mine)
        def _():
            w_row = lax.div(z, 4) * 512 + lax.rem(z, 2) * 256 + y * 64
            w[rows(w_row, 64), :] = wsrc[j]

    x_up, x_down = wrap(x + 1, 4), wrap(x - 1, 4)
    y_up, y_down = wrap(y + 1, 4), wrap(y - 1, 4)
    z_up, z_down = wrap(z + 1, NZ), wrap(z - 1, NZ)
    streams = (
        (at(x_up, y, z, c), at(x, y_up, z, c), 1, True),
        (at(x_down, y, z, c), at(x, y_down, z, c), -1, True),
        (at(x, y_up, z, c), at(x_up, y, z, c), 1, False),
        (at(x, y_down, z, c), at(x_down, y, z, c), -1, False),
    )

    def x_hop(hop):
        for q, (first, second, sign, x_first) in enumerate(streams):
            for i in range(4):
                j = hop - i
                if j < 0 or j > 3:
                    continue
                dx, dy = (i, j) if x_first else (j, i)
                xx, yy = wrap(x - sign * dx, 4), wrap(y - sign * dy, 4)
                place = xg.at[
                    rows(yy * TOK + 64 * q, 64),
                    pl.ds(pl.multiple_of(xx * 512, 512), 512),
                ]
                source = xin.at[pl.ds(64 * q, 64), :] if hop == 0 else place
                if hop:
                    remote(
                        place, place, x_send2.at[q, 4 * i], x_recv.at[q, 4 * i + j], first
                    ).wait_recv()
                if j == 0 and i < 3:
                    start(
                        remote(
                            source, place, x_send1.at[q, i], x_recv.at[q, 4 * i + 4], first
                        )
                    )
                if j < 3:
                    start(
                        remote(
                            source,
                            place,
                            x_send2.at[q, 4 * i + j],
                            x_recv.at[q, 4 * i + j + 1],
                            second,
                        )
                    )

    x_hop(0)

    def ow_at(zz, xx):
        at_row = (4 * lax.rem(zz, 4) + y) * 64
        return ow.at[rows(at_row, 64), pl.ds(pl.multiple_of(xx * 256, 256), 256)]

    z_quarter = lax.div(z, 4)
    start(
        remote(owsrc, ow_at(z, x), ox_send, ox_recv.at[x], at(z_quarter, y, z, c)),
        x != z_quarter,
    )

    @pl.when(x == z_quarter)
    def _():
        ow[
            rows((4 * lax.rem(z, 4) + y) * 64, 64), pl.ds(pl.multiple_of(x * 256, 256), 256)
        ] = owsrc[...]

    for j in range(2):
        mine = jnp.logical_and(2 * c + j == y, y_half == c)
        start(
            remote(
                exsrc.at[j],
                exb.at[y_low],
                ex_send.at[j],
                ex_recv.at[y_low],
                at(x, 2 * c + j, z, y_half),
            ),
            jnp.logical_not(mine),
        )

        @pl.when(mine)
        def _():
            exb[y_low] = exsrc[j]

    up, down = (z_up, y, t), (z_down, y, t)

    def w_hop(d):
        if d == 0:
            mine = z_class == c
            for k in range(4):
                here = w_at(z, k)
                local = jnp.logical_and(y == k, y_half == c)

                @pl.when(jnp.logical_and(mine, jnp.logical_not(local)))
                def _():
                    remote(here, here, wy_send.at[0], wy_recv.at[k], up).wait_recv()

                start(remote(here, here, wz_send.at[0, 0, k], wz_recv.at[0, 1, k], up), mine)
                start(
                    remote(here, here, wz_send.at[1, 0, k], wz_recv.at[1, 1, k], down), mine
                )
            return
        for way, (target, far, last) in enumerate(((up, z - d, 8), (down, z + d, 7))):
            if d > last:
                continue
            origin = wrap(far, NZ)
            mine = lax.rem(lax.div(origin, 2), 2) == c
            for k in range(4):
                here = w_at(origin, k)
                copy = remote(
                    here, here, wz_send.at[way, d, k], wz_recv.at[way, d + 1, k], target
                )
                arrived = remote(
                    here, here, wz_send.at[way, d, k], wz_recv.at[way, d, k], target
                )
                pl.when(mine)(arrived.wait_recv)
                if d < last:
                    start(copy, mine)

    def ow_hop(d):
        if d == 0:
            mine = x == z_quarter
            for k in range(4):
                here = ow_at(z, k)

                @pl.when(jnp.logical_and(mine, x != k))
                def _():
                    remote(here, here, ox_send, ox_recv.at[k], up).wait_recv()

                start(remote(here, here, oz_send.at[0, 0, k], oz_recv.at[0, 1, k], up), mine)
                start(
                    remote(here, here, oz_send.at[1, 0, k], oz_recv.at[1, 1, k], down), mine
                )
            return
        for way, (target, far, last) in enumerate(((up, z - d, 8), (down, z + d, 7))):
            if d > last:
                continue
            origin = wrap(far, NZ)
            mine = lax.div(origin, 4) == x
            for k in range(4):
                here = ow_at(origin, k)
                copy = remote(
                    here, here, oz_send.at[way, d, k], oz_recv.at[way, d + 1, k], target
                )
                arrived = remote(
                    here, here, oz_send.at[way, d, k], oz_recv.at[way, d, k], target
                )
                pl.when(mine)(arrived.wait_recv)
                if d < last:
                    start(copy, mine)

    w_hop(0)
    ow_hop(0)

    lane = iota((TOK, TOK), 1)
    row = iota((TOK, TOK), 0)
    xors[...] = jnp.bitwise_xor(row, lane)
    one = jnp.ones((TOK, TOK), F32)
    nil = jnp.zeros((TOK, TOK), F32)

    def level_matrix(level, carry):
        half = lax.shift_left(jnp.int32(1), level)
        base = lane - jnp.bitwise_and(lane, 2 * half - 1)
        middle = base + half - 1
        low = jnp.minimum(lane, middle)
        high = jnp.maximum(lane, middle)
        mats[level] = jnp.where(
            jnp.logical_and(row > low, row <= high), one, nil
        ).astype(BF16)
        return carry

    lax.fori_loop(0, 8, level_matrix, 0)
    mats[8] = jnp.where(row <= lane, one, nil).astype(BF16)
    mats[9] = jnp.where(row > lane, one, nil).astype(BF16)

    for hop in range(1, 10):
        if hop <= 6:
            x_hop(hop)
        if hop <= 8:
            w_hop(hop)
        if hop >= 2:
            ow_hop(hop - 1)

    def project(half, target):
        def tile(s, carry):
            block = xg[rows((2 * half + s) * TOK, TOK), :]
            target[rows(s * TOK, TOK), :384] = jnp.dot(
                block, w[...], preferred_element_type=F32
            )
            squares = jnp.zeros((TOK, 128), F32)
            for k in range(16):
                piece = block[:, 128 * k : 128 * k + 128].astype(F32)
                squares = squares + piece * piece
            target[rows(s * TOK, TOK), 384:] = squares
            return carry

        lax.fori_loop(0, 2, tile, 0)

    project(1 - c, acc_send)
    swap = remote(acc_send, acc_recv, d2d_send.at[0], d2d_recv.at[0], partner)
    start(swap)
    project(c, acc_own)
    swap.wait_recv()

    low_lanes = iota((TOK, 128), 1) < 64

    def scaled(s):
        both = acc_own[rows(s * TOK, TOK), :] + acc_recv[rows(s * TOK, TOK), :]
        mean = jnp.sum(both[:, 384:], axis=1, keepdims=True) * (1.0 / 4096.0)
        factor = lax.rsqrt(mean + 1e-06)
        return (both[:, :384] * factor).astype(BF16).astype(F32)

    p0, p1 = scaled(0), scaled(1)

    first, second = p0[:, :128], p1[:, :128]
    left = jnp.where(low_lanes, first, roll64(second))
    right = jnp.where(low_lanes, roll64(first), second)
    ext[32:, :] = (left * sigmoid(right)).astype(BF16).astype(F32)
    start(
        remote(
            ext.at[pl.ds(TOK, 32), :], ext.at[pl.ds(0, 32), :], halo_send, halo_recv, up
        ),
        z < NZ - 1,
    )

    v0, v1 = p0[:, 128:256], p1[:, 128:256]
    gates = jnp.where(low_lanes, roll64(v0), v1)
    zero = jnp.zeros((TOK, 128), F32)
    v0 = jnp.where(low_lanes, v0, zero).astype(BF16)
    v1 = jnp.where(low_lanes, zero, roll64(v1)).astype(BF16)
    qt0, qt1 = p0[:, 256:].T, p1[:, 256:].T
    queries = jnp.concatenate([qt0[:32], qt1[:32]], axis=0) * (32.0 ** (-0.5))
    keys = jnp.concatenate([qt0[32:64], qt1[32:64]], axis=0)
    for s in range(2):
        local = jnp.logical_and(y_half == c, y_low == s)

        @pl.when(jnp.logical_not(local))
        def _():
            remote(exb.at[s], exb.at[s], ex_send.at[s], ex_recv.at[s], up).wait_recv()

    decays = []
    for s, qt in enumerate((qt0, qt1)):
        pre = (
            jnp.dot(dwt[...], qt[64:].astype(BF16), preferred_element_type=F32) + bias[...]
        )
        log_sig = jnp.minimum(pre, 0.0) - jnp.log1p(jnp.exp(-jnp.abs(pre)))
        decays.append(log_sig * (1.0 / 16.0) + exb[s])
    decay = jnp.concatenate(decays, axis=0)
    part0 = decay.astype(BF16)
    rest = decay - part0.astype(F32)
    part1 = rest.astype(BF16)
    part2 = (rest - part1.astype(F32)).astype(BF16)
    parts = jnp.concatenate([part0, part1, part2], axis=0)

    def decay_sums(which):
        sums = jnp.dot(parts, mats[which], preferred_element_type=F32)
        return jnp.exp(sums[:64] + sums[64:128] + sums[128:])

    tail_keys = (keys * decay_sums(9)).astype(BF16)
    st_me[...] = (
        jnp.dot(tail_keys[:32], v0, preferred_element_type=F32)
        + jnp.dot(tail_keys[32:], v1, preferred_element_type=F32)
    ).astype(BF16)
    wide = jnp.concatenate([decay, jnp.zeros((64, TOK), F32)], axis=0)
    tot_me[...] = lax.dot_general(
        jnp.ones((8, TOK), F32), wide, NT, precision=HIGHEST, preferred_element_type=F32
    )[:1]

    def tell(k, carry):
        @pl.when(z + k < NZ)
        def _():
            there = (z + k, y, t)
            remote(tot_me, tots.at[z], tot_send.at[k], tot_recv.at[z], there).start()
            remote(st_me, sts.at[z], st_send.at[k], st_recv.at[z], there).start()

        return carry

    lax.fori_loop(1, NZ, tell, 0)

    @pl.when(z == 0)
    def _():
        ext[:32, :] = jnp.zeros((32, 128), F32)

    @pl.when(z > 0)
    def _():
        halo = ext.at[pl.ds(0, 32), :]
        remote(halo, halo, halo_send, halo_recv, up).wait_recv()

    conv = jnp.zeros((TOK, 128), F32)
    for tap in range(31):
        conv = conv + taps[tap : tap + 1, :] * ext[2 + tap : 2 + tap + TOK, :]
    lane8, row8 = iota((8, 128), 1), iota((8, 128), 0)
    seq_of = lax.div(lane8, 64)
    pick_sum = jnp.where(row8 == seq_of, 1.0, 0.0).astype(F32)
    pick_square = jnp.where(row8 == seq_of + 2, 1.0, 0.0).astype(F32)
    me = 4 * x + y
    stats[me] = lax.dot_general(
        pick_sum, conv, NT, precision=HIGHEST, preferred_element_type=F32
    ) + lax.dot_general(
        pick_square, conv * conv, NT, precision=HIGHEST, preferred_element_type=F32
    )

    def stat_copy(k):
        other = lax.rem(me + k, 16)
        xx = lax.div(other, 4)
        return remote(
            stats.at[me],
            stats.at[me],
            stat_send.at[k],
            stat_recv.at[me],
            at(xx, other - 4 * xx, z, c),
        )

    def send_stat(k, carry):
        stat_copy(k).start()
        return carry

    lax.fori_loop(1, 16, send_stat, 0)

    y_next, y_prev = at(x, y_up, z, c), at(x, y_down, z, c)

    def oy_at(k, yy):
        return ow.at[rows((4 * k + yy) * 64, 64), :]

    for k in range(4):
        here = oy_at(k, y)
        start(remote(here, here, oy_send.at[0, k], oy_recv.at[0, k], y_next))
        start(remote(here, here, oy_send.at[1, k], oy_recv.at[1, k], y_prev))

    queries_low, keys_low = queries.astype(BF16), keys.astype(BF16)
    for s in range(2):
        own = lax.dot_general(
            queries_low[32 * s : 32 * s + 32],
            keys_low[32 * s : 32 * s + 32],
            TN,
            preferred_element_type=F32,
        )
        scores[s] = jnp.where(xors[...] == 0, own, 0.0)
    lane64 = iota((64, TOK), 1)

    def level_scores(level, carry):
        factor = decay_sums(level)
        upper = jnp.bitwise_and(lax.shift_right_logical(lane64, level), 1) == 1
        q_level = jnp.where(upper, queries * factor, 0.0).astype(BF16)
        k_level = jnp.where(upper, 0.0, keys * factor).astype(BF16)
        same = lax.shift_right_logical(xors[...], level + 1) == 0
        for s in range(2):
            pair = lax.dot_general(
                q_level[32 * s : 32 * s + 32],
                k_level[32 * s : 32 * s + 32],
                TN,
                preferred_element_type=F32,
            )
            scores[s] = scores[s] + jnp.where(same, pair, 0.0)
        return carry

    lax.fori_loop(0, 8, level_scores, 0)
    heads = jnp.dot(scores[0].astype(BF16), v0, preferred_element_type=F32) + jnp.dot(
        scores[1].astype(BF16), v1, preferred_element_type=F32
    )
    q_start = (queries * decay_sums(8)).astype(BF16)

    def wait_stat(k, carry):
        other = lax.rem(me + k, 16)
        there = stats.at[other]
        remote(there, there, stat_send.at[k], stat_recv.at[other], up).wait_recv()
        return carry

    lax.fori_loop(1, 16, wait_stat, 0)
    total = stats[0]
    for k in range(1, 16):
        total = total + stats[k]
    average = lax.dot_general(
        total, pick_sum * (1.0 / 1024.0), TN, precision=HIGHEST, preferred_element_type=F32
    )
    spread = lax.dot_general(
        total, pick_square * (1.0 / 1024.0), TN, precision=HIGHEST, preferred_element_type=F32
    )
    variance = jnp.maximum(spread - average * average, 0.0)
    normed = (conv - average) * lax.rsqrt(variance + 1e-05) * cgain[...]
    conv_act = normed * sigmoid(normed)

    for k in range(NZ - 1):

        @pl.when(k < z)
        def _():
            remote(
                tots.at[k], tots.at[k], tot_send.at[0], tot_recv.at[k], up
            ).wait_recv()
            remote(sts.at[k], sts.at[k], st_send.at[0], st_recv.at[k], up).wait_recv()

    row16 = iota((NZ, 128), 0)
    known = jnp.where(row16 < z, tots[:, 0, :], 0.0)
    from_row, to_row = iota((NZ, NZ), 0), iota((NZ, NZ), 1)
    between = jnp.where(
        jnp.logical_and(to_row > from_row, to_row < z), 1.0, 0.0
    ).astype(F32)
    exponent = jnp.dot(between, known, precision=HIGHEST, preferred_element_type=F32)
    reach = jnp.where(row16 < z, jnp.exp(exponent), 0.0)
    reach = jnp.concatenate([reach, jnp.zeros((128 - NZ, 128), F32)], axis=0).T
    low32 = iota((32, 128), 1) < 64
    entering = jnp.zeros((32, 128), F32)
    for k in range(NZ - 1):
        factor = jnp.where(low32, reach[:32, k : k + 1], reach[32:64, k : k + 1])
        state = jnp.where(z > k, sts[k].astype(F32), 0.0)
        entering = entering + factor * state
    heads = (
        heads
        + lax.dot_general(
            q_start[:32],
            jnp.where(low32, entering, 0.0).astype(BF16),
            TN,
            preferred_element_type=F32,
        )
        + lax.dot_general(
            q_start[32:],
            jnp.where(low32, 0.0, entering).astype(BF16),
            TN,
            preferred_element_type=F32,
        )
    )
    same_head = lax.div(iota((128, 128), 0), 64) == lax.div(iota((128, 128), 1), 64)
    mean_square = jnp.dot(
        heads * heads,
        jnp.where(same_head, 1.0 / 64.0, 0.0).astype(F32),
        precision=HIGHEST,
        preferred_element_type=F32,
    )
    gla_act = (
        heads * lax.rsqrt(mean_square + 1e-06) * hgain[...] * (gates * sigmoid(gates))
    )

    act_me[0] = jnp.where(low_lanes, conv_act, roll64(gla_act)).astype(BF16)
    act_me[1] = jnp.where(low_lanes, roll64(conv_act), gla_act).astype(BF16)
    act_cols = pl.ds(pl.multiple_of(x * 256 + y_low * 128, 128), 128)
    for s in range(2):
        for k in range(4):
            mine = (
                (x == k) & (2 * c + s == y) & (y_half == c)
            )
            start(
                remote(
                    act_me.at[s],
                    acts.at[:, act_cols],
                    act_send.at[s, k],
                    act_recv.at[2 * x + y_low],
                    at(k, 2 * c + s, z, y_half),
                ),
                jnp.logical_not(mine),
            )

            @pl.when(mine)
            def _():
                acts[:, act_cols] = act_me[s]

    def oy_wait(way, k, yy):
        here = oy_at(k, yy)
        remote(here, here, oy_send.at[0, 0], oy_recv.at[way, k], y_next).wait_recv()

    y_far = wrap(y + 2, 4)
    for k in range(2):
        oy_wait(0, k, y_down)
        here = oy_at(k, y_down)
        start(remote(here, here, oy_send.at[2, k], oy_recv.at[2, k], y_next))
        oy_wait(1, k + 2, y_up)
        here = oy_at(k + 2, y_up)
        start(remote(here, here, oy_send.at[2, k + 2], oy_recv.at[2, k + 2], y_prev))
    for k in range(2):
        oy_wait(0, k + 2, y_down)
        oy_wait(1, k, y_up)
    for k in range(4):
        oy_wait(2, k, y_far)

    for k in range(4):
        for j in range(2):
            local = (x == k) & (y_low == j) & (y_half == c)

            @pl.when(jnp.logical_not(local))
            def _():
                here = acts.at[:, pl.ds(256 * k + 128 * j, 128)]
                remote(
                    here, here, act_send.at[0, 0], act_recv.at[2 * k + j], up
                ).wait_recv()

    def output(half):
        return lax.dot_general(
            acts[...], ow[rows(half * 512, 512), :], NT, preferred_element_type=F32
        )

    po_send[...] = output(1 - c).astype(BF16)
    trade = remote(po_send, po_recv, d2d_send.at[1], d2d_recv.at[1], partner)
    start(trade)
    result = xin[...].astype(F32) + output(c)
    trade.wait_recv()
    out[...] = (result + po_recv[...].astype(F32)).astype(BF16)

    for copy, cond in finish:
        if cond is None:
            copy.wait_send()
        else:
            pl.when(cond)(copy.wait_send)

    def told(k, carry):
        @pl.when(z + k < NZ)
        def _():
            there = (z + k, y, t)
            remote(tot_me, tots.at[z], tot_send.at[k], tot_recv.at[z], there).wait_send()
            remote(st_me, sts.at[z], st_send.at[k], st_recv.at[z], there).wait_send()

        return carry

    lax.fori_loop(1, NZ, told, 0)

    def sent_stat(k, carry):
        stat_copy(k).wait_send()
        return carry

    lax.fori_loop(1, 16, sent_stat, 0)


def shards(
    inputs,
    norm_gain,
    conv_in_a,
    conv_in_b,
    query_w,
    key_w,
    value_w,
    out_gate_w,
    pointwise_w,
    gla_out_w,
    forget_first_factor,
    decay_w,
    decay_bias,
    decay_extra,
    conv_kernel,
    conv_gain,
    head_gain,
):
    z, y, t = lax.axis_index("sp"), lax.axis_index("fs"), lax.axis_index("tp")
    group = 4 * (t // 2) + y
    at_row = (4 * z + y) * 64
    gain = lax.dynamic_slice_in_dim(norm_gain, at_row, 64)[:, None, None]
    low_rank = lax.dynamic_slice_in_dim(forget_first_factor, at_row, 64)
    pieces = [
        a.reshape(64, 2, -1)
        for a in (conv_in_a, conv_in_b, value_w, out_gate_w, query_w, key_w)
    ]
    pieces.append(jnp.broadcast_to(low_rank[:, None, :], (64, 2, 64)))
    packed = jnp.concatenate(pieces, axis=2).astype(F32) * gain
    wsrc = packed.astype(BF16).transpose(1, 0, 2)
    owsrc = jnp.concatenate(
        [pointwise_w.reshape(64, 2, 64), gla_out_w.reshape(64, 2, 64)], axis=2
    ).reshape(64, 256)
    exsrc = decay_extra[0].T.reshape(2, 32, TOK)
    dwt = lax.dynamic_slice_in_dim(decay_w, group * 32, 32, 1).T
    bias = lax.dynamic_slice_in_dim(decay_bias, group * 32, 32)[:, None]
    taps = jnp.tile(lax.dynamic_slice_in_dim(conv_kernel, group * 64, 64, 1), (1, 2))
    cgain = jnp.tile(lax.dynamic_slice_in_dim(conv_gain, group * 64, 64), 2)[None]
    hgain = jnp.tile(head_gain, 2)[None]

    dma = pltpu.SemaphoreType.DMA
    vmem = pltpu.VMEM
    mixed = pl.pallas_call(
        body,
        out_shape=jax.ShapeDtypeStruct((TOK, 512), BF16),
        in_specs=[pl.BlockSpec(memory_space=vmem)] * 9,
        out_specs=pl.BlockSpec(memory_space=vmem),
        scratch_shapes=[
            vmem((4 * TOK, 2048), BF16),
            vmem((2048, 384), BF16),
            vmem((1024, 1024), BF16),
            vmem((512, 512), F32),
            vmem((512, 512), F32),
            vmem((512, 512), F32),
            vmem((10, TOK, TOK), BF16),
            vmem((TOK, TOK), jnp.int32),
            vmem((2, TOK, TOK), F32),
            vmem((TOK + 32, 128), F32),
            vmem((2, 32, TOK), F32),
            vmem((16, 8, TOK), F32),
            vmem((1, 128), F32),
            vmem((NZ, 1, 128), F32),
            vmem((32, 128), BF16),
            vmem((NZ, 32, 128), BF16),
            vmem((2, TOK, 128), BF16),
            vmem((TOK, 1024), BF16),
            vmem((TOK, 512), BF16),
            vmem((TOK, 512), BF16),
            dma((4, 4)),
            dma((4, 16)),
            dma((4, 16)),
            dma((2,)),
            dma((4,)),
            dma((2, 9, 4)),
            dma((2, 9, 4)),
            dma,
            dma((4,)),
            dma((2, 9, 4)),
            dma((2, 9, 4)),
            dma((3, 4)),
            dma((3, 4)),
            dma((2,)),
            dma((2,)),
            dma((2,)),
            dma((2,)),
            dma,
            dma,
            dma((16,)),
            dma((16,)),
            dma((16,)),
            dma((16,)),
            dma((16,)),
            dma((16,)),
            dma((2, 4)),
            dma((8,)),
        ],
        compiler_params=pltpu.CompilerParams(
            collective_id=0, has_side_effects=True, vmem_limit_bytes=48 * 1024 * 1024
        ),
        name="mixer",
    )(inputs[0], wsrc, owsrc, exsrc, dwt, bias, taps, cgain, hgain)
    return mixed[None]


def solution(mesh):
    weights = P(("sp", "fs"), "tp")
    return jax.shard_map(
        shards,
        mesh=mesh,
        in_specs=(
            P("fs", "sp", "tp"),
            P(),
            weights,
            weights,
            weights,
            weights,
            weights,
            weights,
            weights,
            weights,
            P(),
            P(),
            P(),
            P("fs", "sp", "tp"),
            P(),
            P(),
            P(),
        ),
        out_specs=P("fs", "sp", "tp"),
        check_vma=False,
    )
```

time: 247 us -> 120 us (0.49)
  the two profiles are of different devices: /device:TPU:1 before, /device:TPU:77 now
where the time goes in v1:
time: 120 us; the launch traced here: 119 us
  Pallas kernels  106 us (88%)
  local copies, waits for them, and re-layouts  12.1 us (10%)
    pallas_call x1, Pallas kernels, shards(): pl.pallas_call(body, out_shape=jax.ShapeDtypeStruct((TOK, 512), BF16), in...  106 us
    unnamed x29, local copies, waits for them, and re-layouts  6.79 us

profile of v1, /device:TPU:77, one launch (start us, length us, event | category | flops | bytes accessed | tf_op | source)
XLA Modules:
  0.0 118.7 jit_solution(3889738642569966991)
XLA Ops:
  0.0 0.0 copy-start
  0.0 0.8 dynamic_slice.19
  0.8 0.8 dynamic-slice_bitcast_fusion
  1.6 0.8 dynamic_slice.23
  2.3 0.0 copy-start.11
  2.3 0.1 broadcast_in_dim_tile.6.cgain
  2.4 0.6 copy-done.11
  3.0 0.1 broadcast_in_dim_tile.7.hgain
  3.1 0.8 constant_dynamic-slice_fusion
  3.9 0.1 tile.9.taps
  4.0 0.8 constant_dynamic-slice_fusion.1
  4.8 0.1 copy.32
  4.9 0.1 copy.31.bias
  4.9 0.0 copy-done
  4.9 0.1 constant_dynamic-slice_fusion.2
  5.0 0.1 copy.23
  5.1 0.0 copy-start.9
  5.2 0.7 copy-done.9
  5.9 0.1 copy.21
  6.0 0.0 copy-start.10
  6.0 0.1 copy.28
  6.1 0.6 copy-done.10
  6.7 0.1 copy.22
  6.8 0.0 copy-start.3
  6.8 0.1 copy.29
  6.9 0.6 copy-done.3
  7.5 0.1 reshape.38
  7.6 0.0 copy-start.4
  7.6 0.7 copy-done.4
  8.3 0.1 reshape.39
  8.4 0.7 copy-done.5
  9.1 0.1 reshape.40
  9.2 0.7 copy-done.6
  9.9 0.1 reshape.41
  10.0 0.0 copy-start.7
  10.0 0.0 copy-start.8
  10.0 0.1 concatenate.6
  10.2 0.0 copy-start.1
  10.2 0.1 fusion.wsrc
  10.3 0.5 copy-done.7
  10.7 0.1 reshape.44
  10.8 0.0 copy-done.8
  10.8 0.1 reshape.45
  10.9 0.1 pad_maximum_fusion
  11.0 0.1 copy-done.1
  11.1 0.6 copy-done.2
  11.8 106.3 %mixer.1 = bf16[256,512]{1,0:T(8,128)(2,1)S(1)} custom-call(bf16[256,512]{1,0:T(8,128)(2,1)S(1)} %bitcast.19, bf16[2,64,384]{2,1,0:T(8,128)(2,1)S(1)} %fusion.wsrc, bf16[64,256]{1,0:T(8,128)(2,1)S(1)} %bitcast.20, f32[2,32,256]{2,1,0:T(8,128)S(1)} %bitcast.21, bf16[32,64]{1,0:T(8,128)(2,1)S(1)} %bitcast.22, f32[32,1]{1,0:T(8,128)S(1)} %copy.31.bias, ...), custom_call_target="tpu_custom_call" | custom-call | tf_op jit(solution)/shard_map/mixer/pallas_call | solution.py:737
  118.0 0.7 copy.37
  (12 shorter events, 0.1 us)
Async XLA Ops:
  0.0 4.9 %copy-start = (bf16[4096,64]{0,1:T(8,128)(2,1)S(1)}, bf16[4096,64]{0,1:T(8,128)(2,1)}, u32[]{:S(2)}) copy-start(bf16[4096,64]{0,1:T(8,128)(2,1)} %param.27) | copy-start | bytes 1572868
  2.3 0.7 copy-start.11
  5.1 0.7 copy-start.9
  6.0 0.7 copy-start.10
  6.8 0.7 copy-start.3
  7.6 0.7 copy-start.4
  8.4 0.7 copy-start.5
  9.2 0.7 copy-start.6
  10.0 0.7 copy-start.7
  10.0 0.8 copy-start.8
  10.2 1.0 copy-start.1
  10.9 0.9 copy-start.2

commit v2 on v1

v2 whole, which is shorter than its diff:
```python
import functools
import heapq

import jax
import jax.numpy as jnp
from jax import lax
from jax.experimental import pallas as pl
from jax.experimental.pallas import tpu as pltpu
from jax.sharding import PartitionSpec as P

MESH = pl.DeviceIdType.MESH
F32 = jnp.float32
BF16 = jnp.bfloat16
HIGHEST = lax.Precision.HIGHEST
NZ = 16
TOK = 256
NT = (((1,), (1,)), ((), ()))
TN = (((0,), (0,)), ((), ()))


def remote(src, dst, send, recv, device):
    return pltpu.make_async_remote_copy(
        src_ref=src,
        dst_ref=dst,
        send_sem=send,
        recv_sem=recv,
        device_id=device,
        device_id_type=MESH,
    )


def wrap(value, size):
    return lax.rem(value + size, size)


def rows(start, size):
    return pl.ds(pl.multiple_of(start, size), size)


def iota(shape, dim):
    return lax.broadcasted_iota(jnp.int32, shape, dim)


def sigmoid(value):
    return 1.0 / (1.0 + jnp.exp(-value))


def roll64(value):
    return pltpu.roll(value, 64, 1)


OFFSETS = (0, -1, 1, 2)
W_HOP = 2.2
OW_START, OW_HOP = 4.0, 3.0


def x_forwards(f, g, u):
    sends = []
    if g == 0:
        if f == 0:
            sends += [(0, 0, 1, 0), (0, 1, 2, 0)]
        elif f < 3 and u == f - 1:
            sends += [(0, u, 3, 0)]
        sends += [(1, 0, f, 1), (1, 1, f, 2)]
    elif g < 3 and u == g - 1:
        sends += [(1, u, f, 3)]
    return sends


def x_order():
    free, queue, done = {}, [], []

    def go(now, half, f, g, u):
        for which, way, ff, gg in x_forwards(f, g, u):
            link = ((which + half) % 2, way)
            free[link] = max(free.get(link, 0.0), now) + 1.4
            heapq.heappush(queue, (free[link] + 1.9, half, ff, gg, u))

    for u in range(2):
        for half in range(2):
            go(0.0, half, 0, 0, u)
    while queue:
        event = heapq.heappop(queue)
        done.append(event)
        go(*event)
    return done


def body(
    xin_hbm,
    gain_hbm,
    a_hbm,
    b_hbm,
    q_hbm,
    k_hbm,
    v_hbm,
    gate_hbm,
    point_hbm,
    gla_hbm,
    low_hbm,
    dw_hbm,
    bias_hbm,
    extra_hbm,
    kernel_hbm,
    cgain_hbm,
    hgain_hbm,
    out,
    gain_in,
    tiles_in,
    narrow_in,
    low_in,
    dw_in,
    bias_in,
    exsrc,
    taps_in,
    cgain_in,
    hgain_in,
    wsrc,
    owsrc,
    dwt,
    bias,
    taps,
    in_sem,
    xg,
    w,
    ow,
    acc_own,
    acc_send,
    acc_recv,
    mats,
    xors,
    scores,
    ext,
    exb,
    stats,
    tot_me,
    tots,
    st_me,
    sts,
    act_me,
    acts,
    po_send,
    po_recv,
    x_send,
    xd_send,
    xd_recv,
    own_send,
    ring_recv,
    wy_send,
    wy_recv,
    wz_send,
    wd_send,
    wd_recv,
    ox_send,
    ox_recv,
    oz_send,
    oz_recv,
    od_send,
    od_recv,
    oy_send,
    oy_recv,
    ex_send,
    ex_recv,
    d2d_send,
    d2d_recv,
    halo_send,
    halo_recv,
    stat_send,
    stat_recv,
    tot_send,
    tot_recv,
    st_send,
    st_recv,
    act_send,
    act_recv,
):
    scope = []

    def mark(name):
        if scope:
            scope.pop().__exit__(None, None, None)
        if name:
            scope.append(jax.named_scope(name))
            scope[0].__enter__()

    z = lax.axis_index("sp")
    y = lax.axis_index("fs")
    t = lax.axis_index("tp")
    x = lax.div(t, 2)
    c = t - 2 * x
    y_half = lax.div(y, 2)
    y_low = y - 2 * y_half
    z_class = lax.rem(lax.div(z, 2), 2)
    partner = (z, y, 2 * x + 1 - c)

    def at(xx, yy, zz, cc):
        return (zz, yy, 2 * xx + cc)

    mark("greet")
    group_pair = 2 * x + y_half

    def tile_of(index):
        return pl.ds(pl.multiple_of(index * 128, 128), 128)

    def feature_cols(xx, cc):
        return pl.ds(pl.multiple_of((2 * xx + cc) * 512, 512), 512)

    fetches = [
        pltpu.make_async_copy(source, target, in_sem.at[k])
        for k, (source, target) in enumerate(
            (
                (a_hbm, tiles_in.at[0]),
                (b_hbm, tiles_in.at[1]),
                (v_hbm, tiles_in.at[2]),
                (gate_hbm, tiles_in.at[3]),
                (point_hbm, tiles_in.at[4]),
                (gla_hbm, tiles_in.at[5]),
                (q_hbm, narrow_in.at[0]),
                (k_hbm, narrow_in.at[1]),
                (gain_hbm, gain_in),
                (low_hbm.at[:, tile_of(2 * z + y_half)], low_in),
                (xin_hbm, xg.at[rows(y * TOK, TOK), feature_cols(x, c)]),
                (extra_hbm, exsrc),
                (dw_hbm.at[:, tile_of(x)], dw_in),
                (bias_hbm, bias_in),
                (kernel_hbm.at[:, tile_of(group_pair)], taps_in),
                (cgain_hbm, cgain_in),
                (hgain_hbm, hgain_in),
            )
        )
    ]
    for fetch in fetches:
        fetch.start()

    barrier = pltpu.get_barrier_semaphore()

    def greet_plane(k, carry):
        flat = lax.rem(y * 8 + t + k, 32)
        yy = lax.div(flat, 8)
        pl.semaphore_signal(
            barrier, inc=1, device_id=(z, yy, flat - 8 * yy), device_id_type=MESH
        )
        return carry

    lax.fori_loop(1, 32, greet_plane, 0)

    for step in (1, NZ - 1):
        pl.semaphore_signal(
            barrier, inc=1, device_id=(lax.rem(z + step, NZ), y, t), device_id_type=MESH
        )

    mark("pack")
    low64 = iota((64, 128), 1) < 64
    lane64 = iota((64, 128), 1)
    y_even = y_low == 0

    def column(row_vector):
        return jnp.broadcast_to(row_vector, (128, 128)).T

    for fetch in fetches[:10]:
        fetch.wait()
    gain_all = column(gain_in[pl.ds(2 * z + y_half, 1), :])
    gain = jnp.where(y_even, gain_all[:64], gain_all[64:])

    def pair(k, scale):
        first = tiles_in[k].astype(F32) * scale
        second = tiles_in[k + 1].astype(F32) * scale
        return (
            jnp.where(low64, first, roll64(second)).astype(BF16),
            jnp.where(low64, roll64(first), second).astype(BF16),
        )

    for k in range(2):
        both = pair(2 * k, gain)
        for j in range(2):
            wsrc[j, :, 128 * k : 128 * k + 128] = both[j]
    both = pair(4, 1.0)
    for j in range(2):
        owsrc[:, 128 * j : 128 * j + 128] = both[j]
    narrow = jnp.concatenate([narrow_in[0], narrow_in[1]], axis=1).astype(F32)
    low_rows = low_in[...].astype(F32)
    low_rows = jnp.concatenate([low_rows, low_rows], axis=0).T
    low_rows = jnp.where(y_even, low_rows[:64], low_rows[64:])
    back32, back64 = pltpu.roll(narrow, 96, 1), roll64(narrow)
    mixed0 = jnp.where(low64, jnp.where(lane64 < 32, narrow, back32), low_rows)
    mixed1 = jnp.where(low64, jnp.where(lane64 < 32, back32, back64), low_rows)
    wsrc[0, :, 256:] = (mixed0 * gain).astype(BF16)
    wsrc[1, :, 256:] = (mixed1 * gain).astype(BF16)
    for fetch in fetches[10:12]:
        fetch.wait()
    mark("barrier_wait")
    pl.semaphore_wait(barrier, 31 + 2)

    finish = []

    def start(copy, cond=None):
        if cond is None:
            copy.start()
        else:
            pl.when(cond)(copy.start)
        finish.append((copy, cond))

    mark("first_sends")
    def w_at(zz, k):
        kind = lax.rem(lax.div(zz, 2), 2)
        begin = kind * 2048 + lax.div(zz, 4) * 512 + lax.rem(zz, 2) * 256 + k * 64
        return w.at[rows(begin, 64), :]

    for j in range(2):
        mine = jnp.logical_and(2 * c + j == y, c == 1)
        start(
            remote(
                wsrc.at[j], w_at(z, y), wy_send.at[j], wy_recv.at[y], at(x, 2 * c + j, z, 1)
            ),
            jnp.logical_not(mine),
        )

        @pl.when(mine)
        def _():
            w_at(z, y)[...] = wsrc[j]

    x_up, x_down = wrap(x + 1, 4), wrap(x - 1, 4)
    y_up, y_down = wrap(y + 1, 4), wrap(y - 1, 4)
    z_up, z_down = wrap(z + 1, NZ), wrap(z - 1, NZ)
    along_x = (at(x_up, y, z, c), at(x_down, y, z, c))
    along_y = (at(x, y_up, z, c), at(x, y_down, z, c))

    def x_rows(yy, half, u):
        return rows(yy * TOK + 128 * half + 64 * u, 64)

    def x_event(half, f, g, u):
        df, dg = OFFSETS[f], OFFSETS[g]
        xx, yy = (x + df, y + dg) if half == 0 else (x + dg, y + df)
        xx, yy = wrap(xx, 4), wrap(yy, 4)
        place = xg.at[
            x_rows(yy, half, u), pl.ds(pl.multiple_of(xx * 1024, 1024), 1024)
        ]
        others = xg.at[x_rows(yy, half, u), feature_cols(xx, 1)]
        slot = 32 * half + 8 * f + 2 * g + u
        if f == 0 and g == 0:
            remote(others, others, x_send, ring_recv.at[slot], partner).wait_recv()
        else:
            remote(place, place, x_send, ring_recv.at[slot], partner).wait_recv()
        first, second = (along_x, along_y) if half == 0 else (along_y, along_x)
        for which, way, ff, gg in x_forwards(f, g, u):
            remote(
                place,
                place,
                x_send,
                ring_recv.at[32 * half + 8 * ff + 2 * gg + u],
                (second if which else first)[way],
            ).start()
        if f or g:
            remote(others, others, xd_send, xd_recv, partner).start()

    @pl.when(c == 1)
    def _():
        for u in range(2):
            for half in range(2):
                mine = xg.at[x_rows(y, half, u), feature_cols(x, 1)]
                remote(
                    mine, mine, own_send, ring_recv.at[32 * half + u], partner
                ).start()

    def ow_rows(zz):
        return rows((4 * lax.rem(zz, 4) + y) * 64, 64)

    def ow_cols(xx):
        return pl.ds(pl.multiple_of(xx * 256, 256), 256)

    z_quarter = lax.div(z, 4)
    ow_mine = jnp.logical_and(x == z_quarter, c == 1)
    start(
        remote(
            owsrc,
            ow.at[c, ow_rows(z), ow_cols(x)],
            ox_send,
            ox_recv.at[c, x],
            at(z_quarter, y, z, 1),
        ),
        jnp.logical_not(ow_mine),
    )

    @pl.when(ow_mine)
    def _():
        ow[1, ow_rows(z), ow_cols(x)] = owsrc[...]

    for j in range(2):
        mine = jnp.logical_and(2 * c + j == y, y_half == c)
        start(
            remote(
                exsrc.at[j],
                exb.at[y_low],
                ex_send.at[j],
                ex_recv.at[y_low],
                at(x, 2 * c + j, z, y_half),
            ),
            jnp.logical_not(mine),
        )

        @pl.when(mine)
        def _():
            exb[y_low] = exsrc[j]

    up, down = (z_up, y, t), (z_down, y, t)

    ways = (up, down)

    def w_on(way, d, k, origin):
        here = w_at(origin, k)
        if d < 8 - way:
            remote(here, here, wz_send, ring_recv.at[4 * origin + k], ways[way]).start()
        if d == 0 and way == 0:
            return

        @pl.when(lax.rem(lax.div(origin, 2), 2) == 0)
        def _():
            remote(here, here, wd_send, wd_recv, partner).start()

    def w_start(k):
        here = w_at(z, k)

        @pl.when(jnp.logical_not(jnp.logical_and(y == k, y_half == 1)))
        def _():
            remote(here, here, wz_send, wy_recv.at[k], up).wait_recv()

        w_on(0, 0, k, z)
        w_on(1, 0, k, z)

    def w_event(way, d, k):
        origin = wrap(z - d if way == 0 else z + d, NZ)
        here = w_at(origin, k)
        remote(here, here, wz_send, ring_recv.at[4 * origin + k], up).wait_recv()
        w_on(way, d, k, origin)

    def ow_on(way, d, k, origin):
        here = ow.at[:, ow_rows(origin), ow_cols(k)]
        ours = ow.at[0, ow_rows(origin), ow_cols(k)]
        which = lax.rem(origin, 4)
        if d < 8 - way:
            remote(
                here, here, oz_send.at[way, which], oz_recv.at[which, k], ways[way]
            ).start()
        if d or way:
            remote(ours, ours, od_send, od_recv.at[which], partner).start()

    def ow_start(k):
        @pl.when(x == z_quarter)
        def _():
            for cc in range(2):
                part = ow.at[cc, ow_rows(z), ow_cols(k)]

                @pl.when(jnp.logical_not(jnp.logical_and(x == k, cc == 1)))
                def _():
                    remote(part, part, ox_send, ox_recv.at[cc, k], up).wait_recv()

            ow_on(0, 0, k, z)
            ow_on(1, 0, k, z)

    def ow_event(way, d, k):
        origin = wrap(z - d if way == 0 else z + d, NZ)

        @pl.when(lax.div(origin, 4) == x)
        def _():
            here = ow.at[:, ow_rows(origin), ow_cols(k)]
            remote(
                here, here, ox_send, oz_recv.at[lax.rem(origin, 4), k], up
            ).wait_recv()
            ow_on(way, d, k, origin)

    mark("params")
    for fetch in fetches[12:]:
        fetch.wait()
    dw_all = dw_in[...].astype(F32)
    dw_all = jnp.concatenate([dw_all, dw_all], axis=0).T
    dwt[...] = dw_all.astype(BF16)
    bias[...] = column(bias_in[pl.ds(x, 1), :])
    low31 = iota((31, 128), 1) < 64
    tap_rows = taps_in[...]
    tap_back = roll64(tap_rows)
    taps[:31, :] = jnp.where(low31 == y_even, tap_rows, tap_back)
    cgain_row = cgain_in[pl.ds(group_pair, 1), :]
    cgain = jnp.where(low31[:1] == y_even, cgain_row, roll64(cgain_row))
    hgain = jnp.concatenate([hgain_in[...], hgain_in[...]], axis=1)

    mark("constants")
    lane = iota((TOK, TOK), 1)
    row = iota((TOK, TOK), 0)
    xors[...] = jnp.bitwise_xor(row, lane)
    one = jnp.ones((TOK, TOK), F32)
    nil = jnp.zeros((TOK, TOK), F32)

    def level_matrix(level, carry):
        half = lax.shift_left(jnp.int32(1), level)
        base = lane - jnp.bitwise_and(lane, 2 * half - 1)
        middle = base + half - 1
        low = jnp.minimum(lane, middle)
        high = jnp.maximum(lane, middle)
        mats[level] = jnp.where(
            jnp.logical_and(row > low, row <= high), one, nil
        ).astype(BF16)
        return carry

    lax.fori_loop(0, 8, level_matrix, 0)
    mats[8] = jnp.where(row <= lane, one, nil).astype(BF16)
    mats[9] = jnp.where(row > lane, one, nil).astype(BF16)

    z_agenda = []
    for way in range(2):
        for d in range(1, 9 - way):
            for k in range(4):
                z_agenda.append((W_HOP * d + 0.5 * k, w_event, (way, d, k)))
                z_agenda.append((OW_START + OW_HOP * d + 0.5 * k, ow_event, (way, d, k)))
    z_agenda.sort(key=lambda entry: entry[0])
    needed = max(n for n, entry in enumerate(z_agenda) if entry[1] is w_event) + 1
    mark("gather")

    @pl.when(c == 0)
    def _():
        for u in range(2):
            for half in range(2):
                x_event(half, 0, 0, u)
        for n, (_, *event) in enumerate(x_order()):
            if n % 15 == 0:
                mark(f"x{n}")
            x_event(*event)
        mark("w_arrive")
        everything = w.at[pl.ds(0, 2048), :]
        remote(everything, everything, wd_send, wd_recv, partner).wait_recv()
        mark(None)

    @pl.when(c == 1)
    def _():
        for k in range(4):
            w_start(k)
        for k in range(4):
            ow_start(k)
        for n, (_, call, event) in enumerate(z_agenda[:needed]):
            if n % 24 == 0:
                mark(f"z{n}")
            call(*event)
        mark("x_arrive")
        everything = xg.at[pl.ds(0, 480), :]
        remote(everything, everything, xd_send, xd_recv, partner).wait_recv()
        mark(None)

    def oy_at(k, yy):
        return ow.at[c, rows((4 * k + yy) * 64, 64), :]

    def oy_own(k):
        for way in range(2):
            kk = (k + 2 * way) % 4
            here = oy_at(kk, y)
            remote(here, here, oy_send, oy_recv.at[way, kk], along_y[way]).start()

    def oy_wait(way, k, yy):
        here = oy_at(k, yy)
        remote(here, here, oy_send, oy_recv.at[way, k], partner).wait_recv()

    def oy_pass(k):
        for way, yy in enumerate((y_down, y_up)):
            kk = k + 2 * way
            oy_wait(way, kk, yy)
            here = oy_at(kk, yy)
            remote(here, here, oy_send, oy_recv.at[2, kk], along_y[way]).start()

    mark("project")
    def project(half, target):
        def tile(s, carry):
            blocks = [
                xg[rows((2 * half + s) * TOK, TOK), feature_cols(k, c)] for k in range(4)
            ]
            total = jnp.dot(blocks[0], w[rows(c * 2048, 512), :], preferred_element_type=F32)
            for k in range(1, 4):
                total = total + jnp.dot(
                    blocks[k],
                    w[rows(c * 2048 + 512 * k, 512), :],
                    preferred_element_type=F32,
                )
            target[rows(s * TOK, TOK), :384] = total
            squares = jnp.zeros((TOK, 128), F32)
            for k in range(16):
                piece = blocks[k // 4][:, 128 * (k % 4) : 128 * (k % 4) + 128].astype(F32)
                squares = squares + piece * piece
            target[rows(s * TOK, TOK), 384:] = squares
            return carry

        lax.fori_loop(0, 2, tile, 0)

    project(1 - c, acc_send)
    swap = remote(acc_send, acc_recv, d2d_send.at[0], d2d_recv.at[0], partner)
    start(swap)
    mark("late_weights")

    @pl.when(c == 1)
    def _():
        for _, call, event in z_agenda[needed:]:
            call(*event)

    @pl.when(c == 0)
    def _():
        for k in range(4):
            unit = oy_at(k, y)
            remote(unit, unit, od_send, od_recv.at[k], partner).wait_recv()

    oy_own(0)
    oy_own(1)
    mark("project2")
    project(c, acc_own)
    mark("swap_wait")
    oy_own(2)
    swap.wait_recv()

    mark("gating")
    low_lanes = iota((TOK, 128), 1) < 64

    def scaled(s):
        both = acc_own[rows(s * TOK, TOK), :] + acc_recv[rows(s * TOK, TOK), :]
        mean = jnp.sum(both[:, 384:], axis=1, keepdims=True) * (1.0 / 4096.0)
        factor = lax.rsqrt(mean + 1e-06)
        return (both[:, :384] * factor).astype(BF16).astype(F32)

    p0, p1 = scaled(0), scaled(1)

    first, second = p0[:, :128], p1[:, :128]
    left = jnp.where(low_lanes, first, roll64(second))
    right = jnp.where(low_lanes, roll64(first), second)
    ext[32:, :] = (left * sigmoid(right)).astype(BF16).astype(F32)
    start(
        remote(
            ext.at[pl.ds(TOK, 32), :], ext.at[pl.ds(0, 32), :], halo_send, halo_recv, up
        ),
        z < NZ - 1,
    )

    mark("decay")
    v0, v1 = p0[:, 128:256], p1[:, 128:256]
    gates = jnp.where(low_lanes, roll64(v0), v1)
    zero = jnp.zeros((TOK, 128), F32)
    v0 = jnp.where(low_lanes, v0, zero).astype(BF16)
    v1 = jnp.where(low_lanes, zero, roll64(v1)).astype(BF16)
    qt0, qt1 = p0[:, 256:].T, p1[:, 256:].T
    queries = jnp.concatenate([qt0[:32], qt1[:32]], axis=0) * (32.0 ** (-0.5))
    keys = jnp.concatenate([qt0[32:64], qt1[32:64]], axis=0)
    for s in range(2):
        local = jnp.logical_and(y_half == c, y_low == s)

        @pl.when(jnp.logical_not(local))
        def _():
            remote(exb.at[s], exb.at[s], ex_send.at[s], ex_recv.at[s], up).wait_recv()

    decays = []
    for s, qt in enumerate((qt0, qt1)):
        pre = (
            jnp.dot(
                dwt[rows(32 * y, 32), :][:, :64],
                qt[64:].astype(BF16),
                preferred_element_type=F32,
            )
            + bias[rows(32 * y, 32), :][:, :1]
        )
        log_sig = jnp.minimum(pre, 0.0) - jnp.log1p(jnp.exp(-jnp.abs(pre)))
        decays.append(log_sig * (1.0 / 16.0) + exb[s])
    decay = jnp.concatenate(decays, axis=0)
    part0 = decay.astype(BF16)
    rest = decay - part0.astype(F32)
    part1 = rest.astype(BF16)
    part2 = (rest - part1.astype(F32)).astype(BF16)
    parts = jnp.concatenate([part0, part1, part2], axis=0)

    def decay_sums(which):
        sums = jnp.dot(parts, mats[which], preferred_element_type=F32)
        return jnp.exp(sums[:64] + sums[64:128] + sums[128:])

    tail_keys = (keys * decay_sums(9)).astype(BF16)
    st_me[...] = (
        jnp.dot(tail_keys[:32], v0, preferred_element_type=F32)
        + jnp.dot(tail_keys[32:], v1, preferred_element_type=F32)
    ).astype(BF16)
    wide = jnp.concatenate([decay, jnp.zeros((64, TOK), F32)], axis=0)
    tot_me[...] = lax.dot_general(
        jnp.ones((8, TOK), F32), wide, NT, precision=HIGHEST, preferred_element_type=F32
    )[:1]

    def tell(k, carry):
        @pl.when(z + k < NZ)
        def _():
            there = (z + k, y, t)
            remote(tot_me, tots.at[z], tot_send.at[k], tot_recv.at[z], there).start()
            remote(st_me, sts.at[z], st_send.at[k], st_recv.at[z], there).start()

        return carry

    lax.fori_loop(1, NZ, tell, 0)

    oy_own(3)
    mark("attention")
    queries_low, keys_low = queries.astype(BF16), keys.astype(BF16)
    for s in range(2):
        own = lax.dot_general(
            queries_low[32 * s : 32 * s + 32],
            keys_low[32 * s : 32 * s + 32],
            TN,
            preferred_element_type=F32,
        )
        scores[s] = jnp.where(xors[...] == 0, own, 0.0)
    lane_of = iota((64, TOK), 1)

    def level_scores(level, carry):
        factor = decay_sums(level)
        upper = jnp.bitwise_and(lax.shift_right_logical(lane_of, level), 1) == 1
        q_level = jnp.where(upper, queries * factor, 0.0).astype(BF16)
        k_level = jnp.where(upper, 0.0, keys * factor).astype(BF16)
        same = lax.shift_right_logical(xors[...], level + 1) == 0
        for s in range(2):
            pair = lax.dot_general(
                q_level[32 * s : 32 * s + 32],
                k_level[32 * s : 32 * s + 32],
                TN,
                preferred_element_type=F32,
            )
            scores[s] = scores[s] + jnp.where(same, pair, 0.0)
        return carry

    lax.fori_loop(0, 4, level_scores, 0)

    mark("halo_wait")
    @pl.when(z == 0)
    def _():
        ext[:32, :] = jnp.zeros((32, 128), F32)

    @pl.when(z > 0)
    def _():
        halo = ext.at[pl.ds(0, 32), :]
        remote(halo, halo, halo_send, halo_recv, up).wait_recv()

    mark("conv")
    conv = jnp.zeros((TOK, 128), F32)
    for tap in range(31):
        conv = conv + taps[tap : tap + 1, :] * ext[2 + tap : 2 + tap + TOK, :]
    lane8, row8 = iota((8, 128), 1), iota((8, 128), 0)
    seq_of = lax.div(lane8, 64)
    pick_sum = jnp.where(row8 == seq_of, 1.0, 0.0).astype(F32)
    pick_square = jnp.where(row8 == seq_of + 2, 1.0, 0.0).astype(F32)
    me = 4 * x + y
    stats[me] = lax.dot_general(
        pick_sum, conv, NT, precision=HIGHEST, preferred_element_type=F32
    ) + lax.dot_general(
        pick_square, conv * conv, NT, precision=HIGHEST, preferred_element_type=F32
    )

    def stat_copy(k):
        other = lax.rem(me + k, 16)
        xx = lax.div(other, 4)
        return remote(
            stats.at[me],
            stats.at[me],
            stat_send,
            stat_recv,
            at(xx, other - 4 * xx, z, c),
        )

    def send_stat(k, carry):
        stat_copy(k).start()
        return carry

    lax.fori_loop(1, 16, send_stat, 0)

    oy_pass(0)

    mark("attention2")
    lax.fori_loop(4, 8, level_scores, 0)
    heads = jnp.dot(scores[0].astype(BF16), v0, preferred_element_type=F32) + jnp.dot(
        scores[1].astype(BF16), v1, preferred_element_type=F32
    )
    q_start = (queries * decay_sums(8)).astype(BF16)
    oy_pass(1)

    mark("stat_wait")
    others = stats.at[pl.ds(0, 15)]
    remote(others, others, stat_send, stat_recv, up).wait_recv()
    mark("norm")
    total = stats[0]
    for k in range(1, 16):
        total = total + stats[k]
    average = lax.dot_general(
        total, pick_sum * (1.0 / 1024.0), TN, precision=HIGHEST, preferred_element_type=F32
    )
    spread = lax.dot_general(
        total, pick_square * (1.0 / 1024.0), TN, precision=HIGHEST, preferred_element_type=F32
    )
    variance = jnp.maximum(spread - average * average, 0.0)
    normed = (conv - average) * lax.rsqrt(variance + 1e-05) * cgain
    conv_act = normed * sigmoid(normed)

    mark("state_wait")
    for k in range(NZ - 1):

        @pl.when(k < z)
        def _():
            remote(
                tots.at[k], tots.at[k], tot_send.at[0], tot_recv.at[k], up
            ).wait_recv()
            remote(sts.at[k], sts.at[k], st_send.at[0], st_recv.at[k], up).wait_recv()

    mark("heads")
    row16 = iota((NZ, 128), 0)
    known = jnp.where(row16 < z, tots[:, 0, :], 0.0)
    from_row, to_row = iota((NZ, NZ), 0), iota((NZ, NZ), 1)
    between = jnp.where(
        jnp.logical_and(to_row > from_row, to_row < z), 1.0, 0.0
    ).astype(F32)
    exponent = jnp.dot(between, known, precision=HIGHEST, preferred_element_type=F32)
    reach = jnp.where(row16 < z, jnp.exp(exponent), 0.0)
    reach = jnp.concatenate([reach, jnp.zeros((128 - NZ, 128), F32)], axis=0).T
    low32 = iota((32, 128), 1) < 64
    entering = jnp.zeros((32, 128), F32)
    for k in range(NZ - 1):
        factor = jnp.where(low32, reach[:32, k : k + 1], reach[32:64, k : k + 1])
        state = jnp.where(z > k, sts[k].astype(F32), 0.0)
        entering = entering + factor * state
    heads = (
        heads
        + lax.dot_general(
            q_start[:32],
            jnp.where(low32, entering, 0.0).astype(BF16),
            TN,
            preferred_element_type=F32,
        )
        + lax.dot_general(
            q_start[32:],
            jnp.where(low32, 0.0, entering).astype(BF16),
            TN,
            preferred_element_type=F32,
        )
    )
    same_head = lax.div(iota((128, 128), 0), 64) == lax.div(iota((128, 128), 1), 64)
    mean_square = jnp.dot(
        heads * heads,
        jnp.where(same_head, 1.0 / 64.0, 0.0).astype(F32),
        precision=HIGHEST,
        preferred_element_type=F32,
    )
    gla_act = (
        heads * lax.rsqrt(mean_square + 1e-06) * hgain * (gates * sigmoid(gates))
    )

    mark("act_send")
    act_me[0] = jnp.where(low_lanes, conv_act, roll64(gla_act)).astype(BF16)
    act_me[1] = jnp.where(low_lanes, roll64(conv_act), gla_act).astype(BF16)
    act_cols = pl.ds(pl.multiple_of(x * 256 + y_low * 128, 128), 128)
    for s in range(2):
        for k in range(4):
            mine = (
                (x == k) & (2 * c + s == y) & (y_half == c)
            )
            copy = remote(
                act_me.at[s],
                acts.at[:, act_cols],
                act_send,
                act_recv,
                at(k, 2 * c + s, z, y_half),
            )
            pl.when(jnp.logical_not(mine))(copy.start)

            @pl.when(mine)
            def _():
                acts[:, act_cols] = act_me[s]

    mark("oy_rest")
    y_far = wrap(y + 2, 4)
    for k in range(2):
        oy_wait(0, k + 2, y_down)
        oy_wait(1, k, y_up)
    for k in range(4):
        oy_wait(2, k, y_far)

    mark("act_wait")
    def act_bytes():
        return acts.at[:, pl.ds(0, 896)], acts

    for piece, cond in zip(act_bytes(), (y_half == c, y_half != c)):

        @pl.when(cond)
        def _():
            remote(piece, piece, act_send, act_recv, up).wait_recv()

    mark("output")
    def output(half):
        return lax.dot_general(
            acts[...], ow[c, rows(half * 512, 512), :], NT, preferred_element_type=F32
        )

    po_send[...] = output(1 - c).astype(BF16)
    trade = remote(po_send, po_recv, d2d_send.at[1], d2d_recv.at[1], partner)
    start(trade)
    residual = xg[rows(y * TOK, TOK), feature_cols(x, c)]
    result = residual.astype(F32) + output(c)
    mark("trade_wait")
    trade.wait_recv()
    out[...] = (result + po_recv[...].astype(F32)).astype(BF16)

    mark("drain")
    for copy, cond in finish:
        if cond is None:
            copy.wait_send()
        else:
            pl.when(cond)(copy.wait_send)

    def told(k, carry):
        @pl.when(z + k < NZ)
        def _():
            there = (z + k, y, t)
            remote(tot_me, tots.at[z], tot_send.at[k], tot_recv.at[z], there).wait_send()
            remote(st_me, sts.at[z], st_send.at[k], st_recv.at[z], there).wait_send()

        return carry

    lax.fori_loop(1, NZ, told, 0)

    def left(piece, semaphore, cond=None):
        copy = remote(piece, piece, semaphore, stat_recv, partner)
        if cond is None:
            copy.wait_send()
        else:
            pl.when(cond)(copy.wait_send)

    left(stats.at[pl.ds(0, 15)], stat_send)
    left(ow.at[c, pl.ds(0, 768), :], oy_send)
    for piece, cond in zip(act_bytes(), (y_half == c, y_half != c)):
        left(piece, act_send, cond)
    left(xg.at[pl.ds(0, 960), :], x_send, c == 0)
    left(xg.at[pl.ds(0, 480), :], xd_send, c == 0)
    left(xg.at[pl.ds(0, 32), :], own_send, c == 1)
    left(w.at[pl.ds(0, 3840), :], wz_send, c == 1)
    left(w.at[pl.ds(0, 2048), :], wd_send, c == 1)
    left(ow.at[0, pl.ds(0, 256), :], od_send, c == 1)
    for way in range(2):
        for k in range(4):
            origin = 4 * x + k
            hops = wrap(z - origin if way == 0 else origin - z, NZ)
            left(
                ow.at[:, pl.ds(0, 64), :],
                oz_send.at[way, k],
                jnp.logical_and(c == 1, hops < 8 - way),
            )
    mark(None)


def shards(
    inputs,
    norm_gain,
    conv_in_a,
    conv_in_b,
    query_w,
    key_w,
    value_w,
    out_gate_w,
    pointwise_w,
    gla_out_w,
    forget_first_factor,
    decay_w,
    decay_bias,
    decay_extra,
    conv_kernel,
    conv_gain,
    head_gain,
):
    dma = pltpu.SemaphoreType.DMA
    vmem = pltpu.VMEM
    mixed = pl.pallas_call(
        body,
        out_shape=jax.ShapeDtypeStruct((TOK, 512), BF16),
        in_specs=[pl.BlockSpec(memory_space=pltpu.HBM)] * 17,
        out_specs=pl.BlockSpec(memory_space=vmem),
        scratch_shapes=[
            vmem((32, 128), F32),
            vmem((6, 64, 128), BF16),
            vmem((2, 64, 64), BF16),
            vmem((64, 128), BF16),
            vmem((64, 128), BF16),
            vmem((4, 128), F32),
            vmem((2, 32, TOK), F32),
            vmem((31, 128), F32),
            vmem((8, 128), F32),
            vmem((1, 64), F32),
            vmem((2, 64, 384), BF16),
            vmem((64, 256), BF16),
            vmem((128, 128), BF16),
            vmem((128, 128), F32),
            vmem((32, 128), F32),
            dma((17,)),
            vmem((4 * TOK, 4096), BF16),
            vmem((4096, 384), BF16),
            vmem((2, 1024, 1024), BF16),
            vmem((512, 512), F32),
            vmem((512, 512), F32),
            vmem((512, 512), F32),
            vmem((10, TOK, TOK), BF16),
            vmem((TOK, TOK), jnp.int32),
            vmem((2, TOK, TOK), F32),
            vmem((TOK + 32, 128), F32),
            vmem((2, 32, TOK), F32),
            vmem((16, 8, TOK), F32),
            vmem((1, 128), F32),
            vmem((NZ, 1, 128), F32),
            vmem((32, 128), BF16),
            vmem((NZ, 32, 128), BF16),
            vmem((2, TOK, 128), BF16),
            vmem((TOK, 1024), BF16),
            vmem((TOK, 512), BF16),
            vmem((TOK, 512), BF16),
            dma,
            dma,
            dma,
            dma,
            dma((64,)),
            dma((2,)),
            dma((4,)),
            dma,
            dma,
            dma,
            dma,
            dma((2, 4)),
            dma((2, 4)),
            dma((4, 4)),
            dma,
            dma((4,)),
            dma,
            dma((3, 4)),
            dma((2,)),
            dma((2,)),
            dma((2,)),
            dma((2,)),
            dma,
            dma,
            dma,
            dma,
            dma((16,)),
            dma((16,)),
            dma((16,)),
            dma((16,)),
            dma,
            dma,
        ],
        compiler_params=pltpu.CompilerParams(
            collective_id=0, has_side_effects=True
        ),
        name="mixer",
    )(
        inputs[0],
        norm_gain.reshape(32, 128),
        conv_in_a,
        conv_in_b,
        query_w,
        key_w,
        value_w,
        out_gate_w,
        pointwise_w,
        gla_out_w,
        forget_first_factor.T,
        decay_w,
        decay_bias.reshape(4, 128),
        decay_extra[0].T.reshape(2, 32, TOK),
        conv_kernel,
        conv_gain.reshape(8, 128),
        head_gain.reshape(1, 64),
    )
    return mixed[None]


def solution(mesh):
    weights = P(("sp", "fs"), "tp")
    return jax.shard_map(
        shards,
        mesh=mesh,
        in_specs=(
            P("fs", "sp", "tp"),
            P(),
            weights,
            weights,
            weights,
            weights,
            weights,
            weights,
            weights,
            weights,
            P(),
            P(),
            P(),
            P("fs", "sp", "tp"),
            P(),
            P(),
            P(),
        ),
        out_specs=P("fs", "sp", "tp"),
        check_vma=False,
    )
```

time: 120 us -> 96.5 us (0.80)
  the two profiles are of different devices: /device:TPU:77 before, /device:TPU:1 now
where the time goes in v2:
time: 96.5 us; the launch traced here: 96.4 us
  Pallas kernels  94.7 us (98%)
  local copies, waits for them, and re-layouts  1.67 us (2%)
    pallas_call x1, Pallas kernels, shards(): pl.pallas_call(body, out_shape=jax.ShapeDtypeStruct((TOK, 512), BF16), in...  94.7 us

profile of v2, /device:TPU:1, one launch (start us, length us, event | category | flops | bytes accessed | tf_op | source)
XLA Modules:
  0.0 96.4 jit_solution(9307456033975379955)
XLA Ops:
  0.0 94.7 %mixer.1 = bf16[256,512]{1,0:T(8,128)(2,1)} custom-call(bf16[256,512]{1,0:T(8,128)(2,1)} %bitcast.14, f32[32,128]{1,0:T(8,128)} %bitcast.16, bf16[64,128]{1,0:T(8,128)(2,1)} %a_hbm.1, bf16[64,128]{1,0:T(8,128)(2,1)} %b_hbm.1, bf16[64,64]{1,0:T(8,128)(2,1)} %q_hbm.1, bf16[64,64]{1,0:T(8,128)(2,1)} %k_hbm.1, bf16[64,128]{1,0:T(8,128)(2,1)} %v_hbm.1, ...), custom_call_target="tpu_custom_call" | custom-call | tf_op jit(solution)/shard_map/mixer/pallas_call | solution.py:971
  94.7 1.7 %copy.19 = bf16[1,256,512]{2,1,0:T(8,128)(2,1)} copy(bf16[1,256,512]{2,1,0:T(8,128)(2,1)} %bitcast.12) | data formatting | bytes 524288

commit v3 on v2

--- a/solution.py
+++ b/solution.py
@@ -50,8 +50,8 @@
 
 
 OFFSETS = (0, -1, 1, 2)
-W_HOP = 2.2
-OW_START, OW_HOP = 4.0, 3.0
+UNIT = (64, 64)
+W_HOP, W_PART = 2.7, 0.55
 
 
 def x_forwards(f, g, u):
@@ -73,8 +73,8 @@
     def go(now, half, f, g, u):
         for which, way, ff, gg in x_forwards(f, g, u):
             link = ((which + half) % 2, way)
-            free[link] = max(free.get(link, 0.0), now) + 1.4
-            heapq.heappush(queue, (free[link] + 1.9, half, ff, gg, u))
+            free[link] = max(free.get(link, 0.0), now) + 1.41 * UNIT[half] / 64
+            heapq.heappush(queue, (free[link] + 2.5, half, ff, gg, u))
 
     for u in range(2):
         for half in range(2):
@@ -124,6 +124,7 @@
     xg,
     w,
     ow,
+    owz,
     acc_own,
     acc_send,
     acc_recv,
@@ -151,7 +152,6 @@
     wz_send,
     wd_send,
     wd_recv,
-    ox_send,
     ox_recv,
     oz_send,
     oz_recv,
@@ -173,6 +173,8 @@
     st_recv,
     act_send,
     act_recv,
+    act2_send,
+    act2_recv,
 ):
     scope = []
 
@@ -197,6 +199,19 @@
         return (zz, yy, 2 * xx + cc)
 
     mark("greet")
+    barrier = pltpu.get_barrier_semaphore()
+
+    def greet(zz, yy, tt):
+        pl.semaphore_signal(barrier, inc=1, device_id=(zz, yy, tt), device_id_type=MESH)
+
+    for step in (1, NZ - 1):
+        greet(lax.rem(z + step, NZ), y, t)
+    for step in range(1, 8):
+        greet(z, y, lax.rem(t + step, 8))
+    for step in range(1, 4):
+        for cc in range(2):
+            greet(z, lax.rem(y + step, 4), 2 * x + cc)
+
     group_pair = 2 * x + y_half
 
     def tile_of(index):
@@ -232,23 +247,6 @@
     for fetch in fetches:
         fetch.start()
 
-    barrier = pltpu.get_barrier_semaphore()
-
-    def greet_plane(k, carry):
-        flat = lax.rem(y * 8 + t + k, 32)
-        yy = lax.div(flat, 8)
-        pl.semaphore_signal(
-            barrier, inc=1, device_id=(z, yy, flat - 8 * yy), device_id_type=MESH
-        )
-        return carry
-
-    lax.fori_loop(1, 32, greet_plane, 0)
-
-    for step in (1, NZ - 1):
-        pl.semaphore_signal(
-            barrier, inc=1, device_id=(lax.rem(z + step, NZ), y, t), device_id_type=MESH
-        )
-
     mark("pack")
     low64 = iota((64, 128), 1) < 64
     lane64 = iota((64, 128), 1)
@@ -289,7 +287,7 @@
     for fetch in fetches[10:12]:
         fetch.wait()
     mark("barrier_wait")
-    pl.semaphore_wait(barrier, 31 + 2)
+    pl.semaphore_wait(barrier, 2 + 7 + 6)
 
     finish = []
 
@@ -322,11 +320,12 @@
     x_up, x_down = wrap(x + 1, 4), wrap(x - 1, 4)
     y_up, y_down = wrap(y + 1, 4), wrap(y - 1, 4)
     z_up, z_down = wrap(z + 1, NZ), wrap(z - 1, NZ)
-    along_x = (at(x_up, y, z, c), at(x_down, y, z, c))
-    along_y = (at(x, y_up, z, c), at(x, y_down, z, c))
+    along_x = (at(x_up, y, z, 0), at(x_down, y, z, 0))
+    along_y = (at(x, y_up, z, 0), at(x, y_down, z, 0))
 
     def x_rows(yy, half, u):
-        return rows(yy * TOK + 128 * half + 64 * u, 64)
+        begin = yy * TOK + 2 * UNIT[0] * half + UNIT[half] * u
+        return pl.ds(pl.multiple_of(begin, 16), UNIT[half])
 
     def x_event(half, f, g, u):
         df, dg = OFFSETS[f], OFFSETS[g]
@@ -338,7 +337,7 @@
         others = xg.at[x_rows(yy, half, u), feature_cols(xx, 1)]
         slot = 32 * half + 8 * f + 2 * g + u
         if f == 0 and g == 0:
-            remote(others, others, x_send, ring_recv.at[slot], partner).wait_recv()
+            place = xg.at[x_rows(yy, half, u), feature_cols(xx, c)]
         else:
             remote(place, place, x_send, ring_recv.at[slot], partner).wait_recv()
         first, second = (along_x, along_y) if half == 0 else (along_y, along_x)
@@ -353,37 +352,17 @@
         if f or g:
             remote(others, others, xd_send, xd_recv, partner).start()
 
+    for u in range(2):
+        for half in range(2):
+            x_event(half, 0, 0, u)
+
+    @pl.when(c == 0)
+    def _():
+        remote(owsrc, owz.at[z, 0], own_send, ox_recv, partner).start()
+
     @pl.when(c == 1)
     def _():
-        for u in range(2):
-            for half in range(2):
-                mine = xg.at[x_rows(y, half, u), feature_cols(x, 1)]
-                remote(
-                    mine, mine, own_send, ring_recv.at[32 * half + u], partner
-                ).start()
-
-    def ow_rows(zz):
-        return rows((4 * lax.rem(zz, 4) + y) * 64, 64)
-
-    def ow_cols(xx):
-        return pl.ds(pl.multiple_of(xx * 256, 256), 256)
-
-    z_quarter = lax.div(z, 4)
-    ow_mine = jnp.logical_and(x == z_quarter, c == 1)
-    start(
-        remote(
-            owsrc,
-            ow.at[c, ow_rows(z), ow_cols(x)],
-            ox_send,
-            ox_recv.at[c, x],
-            at(z_quarter, y, z, 1),
-        ),
-        jnp.logical_not(ow_mine),
-    )
-
-    @pl.when(ow_mine)
-    def _():
-        ow[1, ow_rows(z), ow_cols(x)] = owsrc[...]
+        owz[z, 1] = owsrc[...]
 
     for j in range(2):
         mine = jnp.logical_and(2 * c + j == y, y_half == c)
@@ -433,40 +412,51 @@
         remote(here, here, wz_send, ring_recv.at[4 * origin + k], up).wait_recv()
         w_on(way, d, k, origin)
 
-    def ow_on(way, d, k, origin):
-        here = ow.at[:, ow_rows(origin), ow_cols(k)]
-        ours = ow.at[0, ow_rows(origin), ow_cols(k)]
-        which = lax.rem(origin, 4)
+    def ow_cols(xx):
+        return pl.ds(pl.multiple_of(xx * 256, 256), 256)
+
+    def ow_at(zz):
+        k = lax.rem(zz, 4)
+        half = lax.div(k, 2)
+        return ow.at[half, rows(y * 128 + (k - 2 * half) * 64, 64), ow_cols(x)]
+
+    def ow_on(way, d, origin):
+        here = owz.at[origin]
         if d < 8 - way:
+            remote(here, here, oz_send, oz_recv.at[origin], ways[way]).start()
+
+    def ow_give(n, carry):
+        turn = lax.div(n, 4)
+        ahead = jnp.where(turn == 2, 3, jnp.where(turn == 3, 2, turn))
+        column = lax.rem(x + ahead, 4)
+        origin = 4 * column + lax.rem(n, 4)
+        behind = lax.rem(4 - ahead, 4)
+        place = ow_at(origin)
+
+        def give(cc):
             remote(
-                here, here, oz_send.at[way, which], oz_recv.at[which, k], ways[way]
+                owz.at[origin, cc], place, od_send, od_recv.at[behind], at(column, y, z, cc)
             ).start()
-        if d or way:
-            remote(ours, ours, od_send, od_recv.at[which], partner).start()
-
-    def ow_start(k):
-        @pl.when(x == z_quarter)
+
+        give(0)
+        pl.when(column != x)(functools.partial(give, 1))
+
+        @pl.when(column == x)
         def _():
-            for cc in range(2):
-                part = ow.at[cc, ow_rows(z), ow_cols(k)]
-
-                @pl.when(jnp.logical_not(jnp.logical_and(x == k, cc == 1)))
-                def _():
-                    remote(part, part, ox_send, ox_recv.at[cc, k], up).wait_recv()
-
-            ow_on(0, 0, k, z)
-            ow_on(1, 0, k, z)
+            place[...] = owz[origin, 1]
+
+        return carry
+
+    def ow_start():
+        remote(owz.at[z, 0], owz.at[z, 0], oz_send, ox_recv, partner).wait_recv()
+        ow_on(0, 0, z)
+        ow_on(1, 0, z)
 
     def ow_event(way, d, k):
         origin = wrap(z - d if way == 0 else z + d, NZ)
-
-        @pl.when(lax.div(origin, 4) == x)
-        def _():
-            here = ow.at[:, ow_rows(origin), ow_cols(k)]
-            remote(
-                here, here, ox_send, oz_recv.at[lax.rem(origin, 4), k], up
-            ).wait_recv()
-            ow_on(way, d, k, origin)
+        here = owz.at[origin]
+        remote(here, here, oz_send, oz_recv.at[origin], up).wait_recv()
+        ow_on(way, d, origin)
 
     mark("params")
     for fetch in fetches[12:]:
@@ -508,18 +498,14 @@
     z_agenda = []
     for way in range(2):
         for d in range(1, 9 - way):
-            for k in range(4):
-                z_agenda.append((W_HOP * d + 0.5 * k, w_event, (way, d, k)))
-                z_agenda.append((OW_START + OW_HOP * d + 0.5 * k, ow_event, (way, d, k)))
+            for k in range(5):
+                call = ow_event if k == 4 else w_event
+                z_agenda.append((W_HOP * d + W_PART * k, call, (way, d, k)))
     z_agenda.sort(key=lambda entry: entry[0])
-    needed = max(n for n, entry in enumerate(z_agenda) if entry[1] is w_event) + 1
     mark("gather")
 
     @pl.when(c == 0)
     def _():
-        for u in range(2):
-            for half in range(2):
-                x_event(half, 0, 0, u)
         for n, (_, *event) in enumerate(x_order()):
             if n % 15 == 0:
                 mark(f"x{n}")
@@ -533,96 +519,106 @@
     def _():
         for k in range(4):
             w_start(k)
-        for k in range(4):
-            ow_start(k)
-        for n, (_, call, event) in enumerate(z_agenda[:needed]):
+        ow_start()
+        for n, (_, call, event) in enumerate(z_agenda):
             if n % 24 == 0:
                 mark(f"z{n}")
             call(*event)
+        lax.fori_loop(0, 16, ow_give, 0)
         mark("x_arrive")
         everything = xg.at[pl.ds(0, 480), :]
         remote(everything, everything, xd_send, xd_recv, partner).wait_recv()
         mark(None)
 
-    def oy_at(k, yy):
-        return ow.at[c, rows((4 * k + yy) * 64, 64), :]
-
-    def oy_own(k):
-        for way in range(2):
-            kk = (k + 2 * way) % 4
-            here = oy_at(kk, y)
-            remote(here, here, oy_send, oy_recv.at[way, kk], along_y[way]).start()
-
-    def oy_wait(way, k, yy):
-        here = oy_at(k, yy)
-        remote(here, here, oy_send, oy_recv.at[way, k], partner).wait_recv()
-
-    def oy_pass(k):
-        for way, yy in enumerate((y_down, y_up)):
-            kk = k + 2 * way
-            oy_wait(way, kk, yy)
-            here = oy_at(kk, yy)
-            remote(here, here, oy_send, oy_recv.at[2, kk], along_y[way]).start()
+    y_next = (at(x, y_up, z, c), at(x, y_down, z, c))
+    y_from = (y_down, y_up)
+    y_far = wrap(y + 2, 4)
+
+    def oy_at(yy, ahead):
+        return ow.at[:, rows(yy * 128, 128), ow_cols(lax.rem(x + ahead, 4))]
+
+    def oy_own(way, ahead):
+        here = oy_at(y, ahead)
+        remote(here, here, oy_send, oy_recv.at[way, ahead], y_next[way]).start()
+
+    def oy_wait(way, ahead, yy):
+        here = oy_at(yy, ahead)
+        remote(here, here, oy_send, oy_recv.at[way, ahead], partner).wait_recv()
+
+    def oy_pass(way, ahead):
+        oy_wait(way, ahead, y_from[way])
+        here = oy_at(y_from[way], ahead)
+        remote(here, here, oy_send, oy_recv.at[2, ahead], y_next[way]).start()
 
     mark("project")
-    def project(half, target):
-        def tile(s, carry):
+    def swap_part(n):
+        part = pl.ds(128, 384) if n == 0 else pl.ds(0, 128)
+        return remote(
+            acc_send.at[:, part], acc_recv.at[:, part], d2d_send.at[n], d2d_recv.at[n], partner
+        )
+
+    def project(half, target, n):
+        begin, size = (128, 256) if n == 0 else (0, 128)
+        for s in range(2):
+            at_rows = pl.ds(s * TOK, TOK)
             blocks = [
                 xg[rows((2 * half + s) * TOK, TOK), feature_cols(k, c)] for k in range(4)
             ]
-            total = jnp.dot(blocks[0], w[rows(c * 2048, 512), :], preferred_element_type=F32)
-            for k in range(1, 4):
+            total = jnp.zeros((TOK, size), F32)
+            for k in range(4):
                 total = total + jnp.dot(
                     blocks[k],
-                    w[rows(c * 2048 + 512 * k, 512), :],
+                    w[rows(c * 2048 + 512 * k, 512), begin : begin + size],
                     preferred_element_type=F32,
                 )
-            target[rows(s * TOK, TOK), :384] = total
+            target[at_rows, begin : begin + size] = total
+            if n:
+                continue
             squares = jnp.zeros((TOK, 128), F32)
             for k in range(16):
                 piece = blocks[k // 4][:, 128 * (k % 4) : 128 * (k % 4) + 128].astype(F32)
                 squares = squares + piece * piece
-            target[rows(s * TOK, TOK), 384:] = squares
-            return carry
-
-        lax.fori_loop(0, 2, tile, 0)
-
-    project(1 - c, acc_send)
-    swap = remote(acc_send, acc_recv, d2d_send.at[0], d2d_recv.at[0], partner)
-    start(swap)
-    mark("late_weights")
-
-    @pl.when(c == 1)
-    def _():
-        for _, call, event in z_agenda[needed:]:
-            call(*event)
-
-    @pl.when(c == 0)
-    def _():
-        for k in range(4):
-            unit = oy_at(k, y)
-            remote(unit, unit, od_send, od_recv.at[k], partner).wait_recv()
-
-    oy_own(0)
-    oy_own(1)
+            target[at_rows, 384:] = squares
+
+    def ow_wait(ahead):
+        unit = ow.at[0, pl.ds(0, 64), :]
+        copy = remote(unit, unit, od_send, od_recv.at[ahead], partner)
+        if ahead:
+            copy.wait_recv()
+        else:
+            pl.when(c == 0)(copy.wait_recv)
+
+    project(1 - c, acc_send, 0)
+    start(swap_part(0))
+    ow_wait(0)
+    oy_own(0, 0)
+    oy_own(1, 0)
     mark("project2")
-    project(c, acc_own)
+    project(c, acc_own, 0)
+    mark("project3")
+    project(1 - c, acc_send, 1)
+    start(swap_part(1))
     mark("swap_wait")
-    oy_own(2)
-    swap.wait_recv()
+    swap_part(0).wait_recv()
+
+    low_lanes = iota((TOK, 128), 1) < 64
+
+    def scaled(s):
+        at_rows = pl.ds(s * TOK, TOK)
+        both = acc_own[at_rows, 128:] + acc_recv[at_rows, 128:]
+        mean = jnp.sum(both[:, 256:], axis=1, keepdims=True) * (1.0 / 4096.0)
+        factor = lax.rsqrt(mean + 1e-06)
+        return factor, (both[:, :256] * factor).astype(BF16).astype(F32)
+
+    (factor0, p0), (factor1, p1) = scaled(0), scaled(1)
 
     mark("gating")
-    low_lanes = iota((TOK, 128), 1) < 64
-
-    def scaled(s):
-        both = acc_own[rows(s * TOK, TOK), :] + acc_recv[rows(s * TOK, TOK), :]
-        mean = jnp.sum(both[:, 384:], axis=1, keepdims=True) * (1.0 / 4096.0)
-        factor = lax.rsqrt(mean + 1e-06)
-        return (both[:, :384] * factor).astype(BF16).astype(F32)
-
-    p0, p1 = scaled(0), scaled(1)
-
-    first, second = p0[:, :128], p1[:, :128]
+    project(c, acc_own, 1)
+    swap_part(1).wait_recv()
+    first, second = (
+        ((acc_own[part, :128] + acc_recv[part, :128]) * factor).astype(BF16).astype(F32)
+        for part, factor in ((pl.ds(0, TOK), factor0), (pl.ds(TOK, TOK), factor1))
+    )
     left = jnp.where(low_lanes, first, roll64(second))
     right = jnp.where(low_lanes, roll64(first), second)
     ext[32:, :] = (left * sigmoid(right)).astype(BF16).astype(F32)
@@ -634,12 +630,12 @@
     )
 
     mark("decay")
-    v0, v1 = p0[:, 128:256], p1[:, 128:256]
+    v0, v1 = p0[:, :128], p1[:, :128]
     gates = jnp.where(low_lanes, roll64(v0), v1)
     zero = jnp.zeros((TOK, 128), F32)
     v0 = jnp.where(low_lanes, v0, zero).astype(BF16)
     v1 = jnp.where(low_lanes, zero, roll64(v1)).astype(BF16)
-    qt0, qt1 = p0[:, 256:].T, p1[:, 256:].T
+    qt0, qt1 = p0[:, 128:].T, p1[:, 128:].T
     queries = jnp.concatenate([qt0[:32], qt1[:32]], axis=0) * (32.0 ** (-0.5))
     keys = jnp.concatenate([qt0[32:64], qt1[32:64]], axis=0)
     for s in range(2):
@@ -682,18 +678,20 @@
         jnp.ones((8, TOK), F32), wide, NT, precision=HIGHEST, preferred_element_type=F32
     )[:1]
 
-    def tell(k, carry):
-        @pl.when(z + k < NZ)
-        def _():
-            there = (z + k, y, t)
-            remote(tot_me, tots.at[z], tot_send.at[k], tot_recv.at[z], there).start()
-            remote(st_me, sts.at[z], st_send.at[k], st_recv.at[z], there).start()
-
+    def tell(n, carry):
+        half = lax.div(n + 1, 2)
+        k = jnp.where(lax.rem(n, 2) == 0, 8 - half, 8 + half)
+        there = (lax.rem(z + k, NZ), y, t)
+        remote(tot_me, tots.at[z], tot_send, tot_recv, there).start()
+        remote(st_me, sts.at[z], st_send, st_recv, there).start()
         return carry
 
-    lax.fori_loop(1, NZ, tell, 0)
-
-    oy_own(3)
+    lax.fori_loop(0, NZ - 1, tell, 0)
+
+    ow_wait(1)
+    oy_own(0, 1)
+    ow_wait(3)
+    oy_own(1, 3)
     mark("attention")
     queries_low, keys_low = queries.astype(BF16), keys.astype(BF16)
     for s in range(2):
@@ -766,7 +764,11 @@
 
     lax.fori_loop(1, 16, send_stat, 0)
 
-    oy_pass(0)
+    ow_wait(2)
+    oy_own(0, 3)
+    oy_own(1, 2)
+    oy_own(0, 2)
+    oy_own(1, 1)
 
     mark("attention2")
     lax.fori_loop(4, 8, level_scores, 0)
@@ -774,35 +776,12 @@
         scores[1].astype(BF16), v1, preferred_element_type=F32
     )
     q_start = (queries * decay_sums(8)).astype(BF16)
-    oy_pass(1)
-
-    mark("stat_wait")
-    others = stats.at[pl.ds(0, 15)]
-    remote(others, others, stat_send, stat_recv, up).wait_recv()
-    mark("norm")
-    total = stats[0]
-    for k in range(1, 16):
-        total = total + stats[k]
-    average = lax.dot_general(
-        total, pick_sum * (1.0 / 1024.0), TN, precision=HIGHEST, preferred_element_type=F32
-    )
-    spread = lax.dot_general(
-        total, pick_square * (1.0 / 1024.0), TN, precision=HIGHEST, preferred_element_type=F32
-    )
-    variance = jnp.maximum(spread - average * average, 0.0)
-    normed = (conv - average) * lax.rsqrt(variance + 1e-05) * cgain
-    conv_act = normed * sigmoid(normed)
 
     mark("state_wait")
-    for k in range(NZ - 1):
-
-        @pl.when(k < z)
-        def _():
-            remote(
-                tots.at[k], tots.at[k], tot_send.at[0], tot_recv.at[k], up
-            ).wait_recv()
-            remote(sts.at[k], sts.at[k], st_send.at[0], st_recv.at[k], up).wait_recv()
-
+    others = tots.at[pl.ds(0, NZ - 1)]
+    remote(others, others, tot_send, tot_recv, up).wait_recv()
+    others = sts.at[pl.ds(0, NZ - 1)]
+    remote(others, others, st_send, st_recv, up).wait_recv()
     mark("heads")
     row16 = iota((NZ, 128), 0)
     known = jnp.where(row16 < z, tots[:, 0, :], 0.0)
@@ -845,54 +824,85 @@
         heads * lax.rsqrt(mean_square + 1e-06) * hgain * (gates * sigmoid(gates))
     )
 
+    mark("stat_wait")
+    others = stats.at[pl.ds(0, 15)]
+    remote(others, others, stat_send, stat_recv, up).wait_recv()
+    mark("norm")
+    total = stats[0]
+    for k in range(1, 16):
+        total = total + stats[k]
+    average = lax.dot_general(
+        total, pick_sum * (1.0 / 1024.0), TN, precision=HIGHEST, preferred_element_type=F32
+    )
+    spread = lax.dot_general(
+        total, pick_square * (1.0 / 1024.0), TN, precision=HIGHEST, preferred_element_type=F32
+    )
+    variance = jnp.maximum(spread - average * average, 0.0)
+    normed = (conv - average) * lax.rsqrt(variance + 1e-05) * cgain
+    conv_act = normed * sigmoid(normed)
+
     mark("act_send")
     act_me[0] = jnp.where(low_lanes, conv_act, roll64(gla_act)).astype(BF16)
     act_me[1] = jnp.where(low_lanes, roll64(conv_act), gla_act).astype(BF16)
-    act_cols = pl.ds(pl.multiple_of(x * 256 + y_low * 128, 128), 128)
+    def act_cols(j):
+        return pl.ds(pl.multiple_of(x * 256 + j * 128, 128), 128)
+
     for s in range(2):
-        for k in range(4):
-            mine = (
-                (x == k) & (2 * c + s == y) & (y_half == c)
-            )
-            copy = remote(
-                act_me.at[s],
-                acts.at[:, act_cols],
-                act_send,
-                act_recv,
-                at(k, 2 * c + s, z, y_half),
-            )
-            pl.when(jnp.logical_not(mine))(copy.start)
-
-            @pl.when(mine)
-            def _():
-                acts[:, act_cols] = act_me[s]
+        mine = (2 * c + s == y) & (y_half == c)
+        copy = remote(
+            act_me.at[s],
+            acts.at[:, act_cols(y_low)],
+            act_send,
+            act_recv.at[y_low],
+            at(x, 2 * c + s, z, y_half),
+        )
+        pl.when(jnp.logical_not(mine))(copy.start)
+
+        @pl.when(mine)
+        def _():
+            acts[:, act_cols(y_low)] = act_me[s]
+
+    mark("act_pass")
+    oy_pass(0, 0)
+    oy_pass(1, 3)
+    oy_pass(0, 1)
+    oy_pass(1, 2)
+    for n, j in enumerate((y_low, 1 - y_low)):
+        block = acts.at[:, act_cols(j)]
+        arrived = remote(block, block, act_send, act_recv.at[j], partner)
+        if n == 0:
+            pl.when(y_half != c)(arrived.wait_recv)
+        else:
+            arrived.wait_recv()
+        for step in (2, 1, 3):
+            there = at(lax.rem(x + step, 4), y, z, c)
+            remote(block, block, act2_send, act2_recv, there).start()
 
     mark("oy_rest")
-    y_far = wrap(y + 2, 4)
-    for k in range(2):
-        oy_wait(0, k + 2, y_down)
-        oy_wait(1, k, y_up)
-    for k in range(4):
-        oy_wait(2, k, y_far)
-
+    for ahead in (3, 2):
+        oy_wait(0, ahead, y_down)
+    for ahead in (0, 1):
+        oy_wait(1, ahead, y_up)
+    for ahead in (0, 3, 1, 2):
+        oy_wait(2, ahead, y_far)
     mark("act_wait")
-    def act_bytes():
-        return acts.at[:, pl.ds(0, 896)], acts
-
-    for piece, cond in zip(act_bytes(), (y_half == c, y_half != c)):
-
-        @pl.when(cond)
-        def _():
-            remote(piece, piece, act_send, act_recv, up).wait_recv()
-
+    others = acts.at[:, pl.ds(0, 768)]
+    remote(others, others, act2_send, act2_recv, partner).wait_recv()
     mark("output")
     def output(half):
-        return lax.dot_general(
-            acts[...], ow[c, rows(half * 512, 512), :], NT, preferred_element_type=F32
-        )
+        whole = lax.dot_general(acts[...], ow[half], NT, preferred_element_type=F32)
+        parts = [whole[:, 128 * yy : 128 * yy + 128] for yy in range(4)]
+        tiles = []
+        for kk in range(2):
+            for even, odd in ((parts[0], parts[1]), (parts[2], parts[3])):
+                if kk == 0:
+                    tiles.append(jnp.where(low_lanes, even, roll64(odd)))
+                else:
+                    tiles.append(jnp.where(low_lanes, roll64(even), odd))
+        return jnp.concatenate(tiles, axis=1)
 
     po_send[...] = output(1 - c).astype(BF16)
-    trade = remote(po_send, po_recv, d2d_send.at[1], d2d_recv.at[1], partner)
+    trade = remote(po_send, po_recv, d2d_send.at[2], d2d_recv.at[2], partner)
     start(trade)
     residual = xg[rows(y * TOK, TOK), feature_cols(x, c)]
     result = residual.astype(F32) + output(c)
@@ -907,17 +917,6 @@
         else:
             pl.when(cond)(copy.wait_send)
 
-    def told(k, carry):
-        @pl.when(z + k < NZ)
-        def _():
-            there = (z + k, y, t)
-            remote(tot_me, tots.at[z], tot_send.at[k], tot_recv.at[z], there).wait_send()
-            remote(st_me, sts.at[z], st_send.at[k], st_recv.at[z], there).wait_send()
-
-        return carry
-
-    lax.fori_loop(1, NZ, told, 0)
-
     def left(piece, semaphore, cond=None):
         copy = remote(piece, piece, semaphore, stat_recv, partner)
         if cond is None:
@@ -926,24 +925,20 @@
             pl.when(cond)(copy.wait_send)
 
     left(stats.at[pl.ds(0, 15)], stat_send)
-    left(ow.at[c, pl.ds(0, 768), :], oy_send)
-    for piece, cond in zip(act_bytes(), (y_half == c, y_half != c)):
-        left(piece, act_send, cond)
-    left(xg.at[pl.ds(0, 960), :], x_send, c == 0)
+    left(tots.at[pl.ds(0, NZ - 1)], tot_send)
+    left(sts.at[pl.ds(0, NZ - 1)], st_send)
+    left(xg.at[pl.ds(0, 192), :], oy_send)
+    left(acts.at[:, pl.ds(0, 128)], act_send, y_half == c)
+    left(acts.at[:, pl.ds(0, 256)], act_send, y_half != c)
+    left(acts.at[:, pl.ds(0, 768)], act2_send)
+    left(xg.at[pl.ds(0, 832), :], x_send, c == 0)
+    left(xg.at[pl.ds(0, 128), :], x_send, c == 1)
     left(xg.at[pl.ds(0, 480), :], xd_send, c == 0)
-    left(xg.at[pl.ds(0, 32), :], own_send, c == 1)
+    left(owsrc, own_send, c == 0)
     left(w.at[pl.ds(0, 3840), :], wz_send, c == 1)
     left(w.at[pl.ds(0, 2048), :], wd_send, c == 1)
-    left(ow.at[0, pl.ds(0, 256), :], od_send, c == 1)
-    for way in range(2):
-        for k in range(4):
-            origin = 4 * x + k
-            hops = wrap(z - origin if way == 0 else origin - z, NZ)
-            left(
-                ow.at[:, pl.ds(0, 64), :],
-                oz_send.at[way, k],
-                jnp.logical_and(c == 1, hops < 8 - way),
-            )
+    left(ow.at[0, pl.ds(0, 448), :], od_send, c == 1)
+    left(owz.at[pl.ds(0, 15)], oz_send, c == 1)
     mark(None)
 
 
@@ -992,7 +987,8 @@
             dma((17,)),
             vmem((4 * TOK, 4096), BF16),
             vmem((4096, 384), BF16),
-            vmem((2, 1024, 1024), BF16),
+            vmem((2, 512, 1024), BF16),
+            vmem((NZ, 2, 64, 256), BF16),
             vmem((512, 512), F32),
             vmem((512, 512), F32),
             vmem((512, 512), F32),
@@ -1021,25 +1017,26 @@
             dma,
             dma,
             dma,
-            dma((2, 4)),
-            dma((2, 4)),
-            dma((4, 4)),
+            dma,
+            dma((NZ,)),
             dma,
             dma((4,)),
             dma,
             dma((3, 4)),
             dma((2,)),
             dma((2,)),
+            dma((3,)),
+            dma((3,)),
+            dma,
+            dma,
+            dma,
+            dma,
+            dma,
+            dma,
+            dma,
+            dma,
+            dma,
             dma((2,)),
-            dma((2,)),
-            dma,
-            dma,
-            dma,
-            dma,
-            dma((16,)),
-            dma((16,)),
-            dma((16,)),
-            dma((16,)),
             dma,
             dma,
         ],

time: 96.5 us -> 75.6 us (0.78)
  Pallas kernels: 94.7 us -> 73.8 us
    pallas_call x1, Pallas kernels: 94.7 us -> 73.8 us  [shards(): pl.pallas_call(body, out_shape=jax.ShapeDtypeStruct((TOK, 512), BF16), in...]
where the time goes in v3:
time: 75.6 us; the launch traced here: 75.5 us
  Pallas kernels  73.8 us (98%)
  local copies, waits for them, and re-layouts  1.67 us (2%)
    pallas_call x1, Pallas kernels, shards(): pl.pallas_call(body, out_shape=jax.ShapeDtypeStruct((TOK, 512), BF16), in...  73.8 us
    unnamed x1, local copies, waits for them, and re-layouts  1.67 us

profile of v3, /device:TPU:1, one launch (start us, length us, event | category | flops | bytes accessed | tf_op | source)
XLA Modules:
  0.0 75.5 jit_solution(16341381217836066855)
XLA Ops:
  0.0 73.8 %mixer.1 = bf16[256,512]{1,0:T(8,128)(2,1)} custom-call(bf16[256,512]{1,0:T(8,128)(2,1)} %bitcast.14, f32[32,128]{1,0:T(8,128)} %bitcast.16, bf16[64,128]{1,0:T(8,128)(2,1)} %a_hbm.1, bf16[64,128]{1,0:T(8,128)(2,1)} %b_hbm.1, bf16[64,64]{1,0:T(8,128)(2,1)} %q_hbm.1, bf16[64,64]{1,0:T(8,128)(2,1)} %k_hbm.1, bf16[64,128]{1,0:T(8,128)(2,1)} %v_hbm.1, ...), custom_call_target="tpu_custom_call" | custom-call | tf_op jit(solution)/shard_map/mixer/pallas_call | solution.py:966
  73.8 1.7 %copy.19 = bf16[1,256,512]{2,1,0:T(8,128)(2,1)} copy(bf16[1,256,512]{2,1,0:T(8,128)(2,1)} %bitcast.12) | data formatting | bytes 524288

commit v4 on v3

--- a/solution.py
+++ b/solution.py
@@ -43,6 +43,13 @@
 
 def sigmoid(value):
     return 1.0 / (1.0 + jnp.exp(-value))
+
+
+def thirds(value):
+    first = value.astype(BF16)
+    rest = value - first.astype(F32)
+    second = rest.astype(BF16)
+    return first, second, (rest - second.astype(F32)).astype(BF16)
 
 
 def roll64(value):
@@ -571,14 +578,14 @@
                     w[rows(c * 2048 + 512 * k, 512), begin : begin + size],
                     preferred_element_type=F32,
                 )
-            target[at_rows, begin : begin + size] = total
+            target[at_rows, begin : begin + size] = total.astype(target.dtype)
             if n:
                 continue
             squares = jnp.zeros((TOK, 128), F32)
             for k in range(16):
                 piece = blocks[k // 4][:, 128 * (k % 4) : 128 * (k % 4) + 128].astype(F32)
                 squares = squares + piece * piece
-            target[at_rows, 384:] = squares
+            target[at_rows, 384:] = squares.astype(target.dtype)
 
     def ow_wait(ahead):
         unit = ow.at[0, pl.ds(0, 64), :]
@@ -605,7 +612,7 @@
 
     def scaled(s):
         at_rows = pl.ds(s * TOK, TOK)
-        both = acc_own[at_rows, 128:] + acc_recv[at_rows, 128:]
+        both = acc_own[at_rows, 128:] + acc_recv[at_rows, 128:].astype(F32)
         mean = jnp.sum(both[:, 256:], axis=1, keepdims=True) * (1.0 / 4096.0)
         factor = lax.rsqrt(mean + 1e-06)
         return factor, (both[:, :256] * factor).astype(BF16).astype(F32)
@@ -616,7 +623,7 @@
     project(c, acc_own, 1)
     swap_part(1).wait_recv()
     first, second = (
-        ((acc_own[part, :128] + acc_recv[part, :128]) * factor).astype(BF16).astype(F32)
+        ((acc_own[part, :128] + acc_recv[part, :128].astype(F32)) * factor).astype(BF16).astype(F32)
         for part, factor in ((pl.ds(0, TOK), factor0), (pl.ds(TOK, TOK), factor1))
     )
     left = jnp.where(low_lanes, first, roll64(second))
@@ -628,7 +635,6 @@
         ),
         z < NZ - 1,
     )
-
     mark("decay")
     v0, v1 = p0[:, :128], p1[:, :128]
     gates = jnp.where(low_lanes, roll64(v0), v1)
@@ -658,11 +664,7 @@
         log_sig = jnp.minimum(pre, 0.0) - jnp.log1p(jnp.exp(-jnp.abs(pre)))
         decays.append(log_sig * (1.0 / 16.0) + exb[s])
     decay = jnp.concatenate(decays, axis=0)
-    part0 = decay.astype(BF16)
-    rest = decay - part0.astype(F32)
-    part1 = rest.astype(BF16)
-    part2 = (rest - part1.astype(F32)).astype(BF16)
-    parts = jnp.concatenate([part0, part1, part2], axis=0)
+    parts = jnp.concatenate(thirds(decay), axis=0)
 
     def decay_sums(which):
         sums = jnp.dot(parts, mats[which], preferred_element_type=F32)
@@ -690,8 +692,54 @@
 
     ow_wait(1)
     oy_own(0, 1)
+    oy_own(1, 1)
+    mark("halo_wait")
+    @pl.when(z == 0)
+    def _():
+        ext[:32, :] = jnp.zeros((32, 128), F32)
+
+    @pl.when(z > 0)
+    def _():
+        halo = ext.at[pl.ds(0, 32), :]
+        remote(halo, halo, halo_send, halo_recv, up).wait_recv()
+
+    mark("conv")
+    conv = jnp.zeros((TOK, 128), F32)
+    for tap in range(31):
+        conv = conv + taps[tap : tap + 1, :] * ext[2 + tap : 2 + tap + TOK, :]
+    lane8, row8 = iota((8, 128), 1), iota((8, 128), 0)
+    seq_of = lax.div(lane8, 64)
+    pick_sum = jnp.where(row8 == seq_of, 1.0, 0.0).astype(BF16)
+    pick_square = jnp.where(row8 == seq_of + 2, 1.0, 0.0).astype(BF16)
+    me = 4 * x + y
+    stats[me] = lax.dot_general(
+        jnp.concatenate([pick_sum] * 3 + [pick_square] * 3, axis=1),
+        jnp.concatenate([*thirds(conv), *thirds(conv * conv)], axis=1),
+        NT,
+        preferred_element_type=F32,
+    )
+
+    def stat_copy(k):
+        other = lax.rem(me + k, 16)
+        xx = lax.div(other, 4)
+        return remote(
+            stats.at[me],
+            stats.at[me],
+            stat_send,
+            stat_recv,
+            at(xx, other - 4 * xx, z, c),
+        )
+
+    def send_stat(k, carry):
+        stat_copy(k).start()
+        return carry
+
+    lax.fori_loop(1, 16, send_stat, 0)
+
     ow_wait(3)
+    oy_own(0, 3)
     oy_own(1, 3)
+
     mark("attention")
     queries_low, keys_low = queries.astype(BF16), keys.astype(BF16)
     for s in range(2):
@@ -722,60 +770,34 @@
 
     lax.fori_loop(0, 4, level_scores, 0)
 
-    mark("halo_wait")
-    @pl.when(z == 0)
-    def _():
-        ext[:32, :] = jnp.zeros((32, 128), F32)
-
-    @pl.when(z > 0)
-    def _():
-        halo = ext.at[pl.ds(0, 32), :]
-        remote(halo, halo, halo_send, halo_recv, up).wait_recv()
-
-    mark("conv")
-    conv = jnp.zeros((TOK, 128), F32)
-    for tap in range(31):
-        conv = conv + taps[tap : tap + 1, :] * ext[2 + tap : 2 + tap + TOK, :]
-    lane8, row8 = iota((8, 128), 1), iota((8, 128), 0)
-    seq_of = lax.div(lane8, 64)
-    pick_sum = jnp.where(row8 == seq_of, 1.0, 0.0).astype(F32)
-    pick_square = jnp.where(row8 == seq_of + 2, 1.0, 0.0).astype(F32)
-    me = 4 * x + y
-    stats[me] = lax.dot_general(
-        pick_sum, conv, NT, precision=HIGHEST, preferred_element_type=F32
-    ) + lax.dot_general(
-        pick_square, conv * conv, NT, precision=HIGHEST, preferred_element_type=F32
-    )
-
-    def stat_copy(k):
-        other = lax.rem(me + k, 16)
-        xx = lax.div(other, 4)
-        return remote(
-            stats.at[me],
-            stats.at[me],
-            stat_send,
-            stat_recv,
-            at(xx, other - 4 * xx, z, c),
-        )
-
-    def send_stat(k, carry):
-        stat_copy(k).start()
-        return carry
-
-    lax.fori_loop(1, 16, send_stat, 0)
-
     ow_wait(2)
-    oy_own(0, 3)
+    oy_own(0, 2)
     oy_own(1, 2)
-    oy_own(0, 2)
-    oy_own(1, 1)
-
     mark("attention2")
     lax.fori_loop(4, 8, level_scores, 0)
     heads = jnp.dot(scores[0].astype(BF16), v0, preferred_element_type=F32) + jnp.dot(
         scores[1].astype(BF16), v1, preferred_element_type=F32
     )
     q_start = (queries * decay_sums(8)).astype(BF16)
+
+    mark("stat_wait")
+    others = stats.at[pl.ds(0, 15)]
+    remote(others, others, stat_send, stat_recv, up).wait_recv()
+    mark("norm")
+    total = stats[0]
+    for k in range(1, 16):
+        total = total + stats[k]
+    picks = jnp.concatenate([pick_sum, pick_square], axis=1)
+    moments = lax.dot_general(
+        jnp.concatenate(thirds(total), axis=0),
+        jnp.concatenate([picks] * 3, axis=0),
+        TN,
+        preferred_element_type=F32,
+    ) * (1.0 / 1024.0)
+    average, spread = moments[:, :128], moments[:, 128:]
+    variance = jnp.maximum(spread - average * average, 0.0)
+    normed = (conv - average) * lax.rsqrt(variance + 1e-05) * cgain
+    conv_act = normed * sigmoid(normed)
 
     mark("state_wait")
     others = tots.at[pl.ds(0, NZ - 1)]
@@ -814,32 +836,15 @@
         )
     )
     same_head = lax.div(iota((128, 128), 0), 64) == lax.div(iota((128, 128), 1), 64)
+    same_head = jnp.where(same_head, 1.0, 0.0).astype(BF16)
     mean_square = jnp.dot(
-        heads * heads,
-        jnp.where(same_head, 1.0 / 64.0, 0.0).astype(F32),
-        precision=HIGHEST,
+        jnp.concatenate(thirds(heads * heads), axis=1),
+        jnp.concatenate([same_head] * 3, axis=0),
         preferred_element_type=F32,
-    )
+    ) * (1.0 / 64.0)
     gla_act = (
         heads * lax.rsqrt(mean_square + 1e-06) * hgain * (gates * sigmoid(gates))
     )
-
-    mark("stat_wait")
-    others = stats.at[pl.ds(0, 15)]
-    remote(others, others, stat_send, stat_recv, up).wait_recv()
-    mark("norm")
-    total = stats[0]
-    for k in range(1, 16):
-        total = total + stats[k]
-    average = lax.dot_general(
-        total, pick_sum * (1.0 / 1024.0), TN, precision=HIGHEST, preferred_element_type=F32
-    )
-    spread = lax.dot_general(
-        total, pick_square * (1.0 / 1024.0), TN, precision=HIGHEST, preferred_element_type=F32
-    )
-    variance = jnp.maximum(spread - average * average, 0.0)
-    normed = (conv - average) * lax.rsqrt(variance + 1e-05) * cgain
-    conv_act = normed * sigmoid(normed)
 
     mark("act_send")
     act_me[0] = jnp.where(low_lanes, conv_act, roll64(gla_act)).astype(BF16)
@@ -990,8 +995,8 @@
             vmem((2, 512, 1024), BF16),
             vmem((NZ, 2, 64, 256), BF16),
             vmem((512, 512), F32),
-            vmem((512, 512), F32),
-            vmem((512, 512), F32),
+            vmem((512, 512), BF16),
+            vmem((512, 512), BF16),
             vmem((10, TOK, TOK), BF16),
             vmem((TOK, TOK), jnp.int32),
             vmem((2, TOK, TOK), F32),

time: 75.6 us -> 74.9 us (level)
  Pallas kernels: 73.8 us -> 73 us
    pallas_call x1, Pallas kernels: 73.8 us -> 73 us  [shards(): pl.pallas_call(body, out_shape=jax.ShapeDtypeStruct((TOK, 512), BF16), in...]
where the time goes in v4:
time: 74.9 us; the launch traced here: 74.7 us
  Pallas kernels  73 us (97%)
  local copies, waits for them, and re-layouts  1.67 us (2%)
    pallas_call x1, Pallas kernels, shards(): pl.pallas_call(body, out_shape=jax.ShapeDtypeStruct((TOK, 512), BF16), in...  73 us
    unnamed x1, local copies, waits for them, and re-layouts  1.67 us

profile of v4, /device:TPU:1, one launch (start us, length us, event | category | flops | bytes accessed | tf_op | source)
XLA Modules:
  0.0 74.7 jit_solution(5016232378093686072)
XLA Ops:
  0.0 73.0 %mixer.1 = bf16[256,512]{1,0:T(8,128)(2,1)} custom-call(bf16[256,512]{1,0:T(8,128)(2,1)} %bitcast.14, f32[32,128]{1,0:T(8,128)} %bitcast.16, bf16[64,128]{1,0:T(8,128)(2,1)} %a_hbm.1, bf16[64,128]{1,0:T(8,128)(2,1)} %b_hbm.1, bf16[64,64]{1,0:T(8,128)(2,1)} %q_hbm.1, bf16[64,64]{1,0:T(8,128)(2,1)} %k_hbm.1, bf16[64,128]{1,0:T(8,128)(2,1)} %v_hbm.1, ...), custom_call_target="tpu_custom_call" | custom-call | tf_op jit(solution)/shard_map/mixer/pallas_call | solution.py:971
  73.0 1.7 %copy.19 = bf16[1,256,512]{2,1,0:T(8,128)(2,1)} copy(bf16[1,256,512]{2,1,0:T(8,128)(2,1)} %bitcast.12) | data formatting | bytes 524288

commit v5 on v4

--- a/solution.py
+++ b/solution.py
@@ -58,7 +58,7 @@
 
 OFFSETS = (0, -1, 1, 2)
 UNIT = (64, 64)
-W_HOP, W_PART = 2.7, 0.55
+W_HOP, W_PART = 2.7, 0.45
 
 
 def x_forwards(f, g, u):
@@ -75,22 +75,46 @@
 
 
 def x_order():
-    free, queue, done = {}, [], []
-
-    def go(now, half, f, g, u):
-        for which, way, ff, gg in x_forwards(f, g, u):
-            link = ((which + half) % 2, way)
-            free[link] = max(free.get(link, 0.0), now) + 1.41 * UNIT[half] / 64
-            heapq.heappush(queue, (free[link] + 2.5, half, ff, gg, u))
-
-    for u in range(2):
-        for half in range(2):
-            go(0.0, half, 0, 0, u)
-    while queue:
-        event = heapq.heappop(queue)
-        done.append(event)
-        go(*event)
-    return done
+    unit, latency, lead = 1.41, 2.5, 1.5
+    free = {(axis, way): 0.0 for axis in range(2) for way in range(2)}
+    waiting = {link: [] for link in free}
+    events, actions, count = [], [], 0
+
+    def left_over(f, g, u):
+        return 0 if not x_forwards(f, g, u) else 1 if g else 2 + (u == f - 1)
+
+    def feed(link, now):
+        if waiting[link] and free[link] <= now + 1e-6:
+            _, _, since, block, send = heapq.heappop(waiting[link])
+            free[link] = now + unit
+            actions.append((max(since, now - lead), len(actions), block, send))
+            heapq.heappush(events, (now + unit, 0, link))
+            _, _, ff, gg = send
+            heapq.heappush(events, (now + unit + latency, 1, (block[0], ff, gg, block[3])))
+
+    def arrive(now, block):
+        nonlocal count
+        half, f, g, u = block
+        for send in x_forwards(f, g, u):
+            link = ((send[0] + half) % 2, send[1])
+            count += 1
+            heapq.heappush(
+                waiting[link], (-left_over(send[2], send[3], u), count, now, block, send)
+            )
+        for link in free:
+            feed(link, now)
+
+    for half in range(2):
+        for u in range(2):
+            arrive(0.0, (half, 0, 0, u))
+    while events:
+        now, kind, what = heapq.heappop(events)
+        if kind:
+            actions.append((now, -1, what, None))
+            arrive(now, what)
+        else:
+            feed(what, now)
+    return [action[2:] for action in sorted(actions, key=lambda entry: entry[:2])]
 
 
 def body(
@@ -334,34 +358,37 @@
         begin = yy * TOK + 2 * UNIT[0] * half + UNIT[half] * u
         return pl.ds(pl.multiple_of(begin, 16), UNIT[half])
 
-    def x_event(half, f, g, u):
+    def x_place(half, f, g, u):
         df, dg = OFFSETS[f], OFFSETS[g]
         xx, yy = (x + df, y + dg) if half == 0 else (x + dg, y + df)
         xx, yy = wrap(xx, 4), wrap(yy, 4)
-        place = xg.at[
-            x_rows(yy, half, u), pl.ds(pl.multiple_of(xx * 1024, 1024), 1024)
-        ]
-        others = xg.at[x_rows(yy, half, u), feature_cols(xx, 1)]
+        cols = pl.ds(pl.multiple_of(xx * 1024, 1024), 1024)
+        if f == 0 and g == 0:
+            cols = feature_cols(xx, c)
+        return (
+            xg.at[x_rows(yy, half, u), cols],
+            xg.at[x_rows(yy, half, u), feature_cols(xx, 1)],
+        )
+
+    def x_send_on(block, send):
+        place, _ = x_place(*block)
+        half, u = block[0], block[3]
+        which, way, ff, gg = send
+        axis = along_x if (which + half) % 2 == 0 else along_y
+        slot = 32 * half + 8 * ff + 2 * gg + u
+        remote(place, place, x_send, ring_recv.at[slot], axis[way]).start()
+
+    def x_wait(block):
+        place, others = x_place(*block)
+        half, f, g, u = block
         slot = 32 * half + 8 * f + 2 * g + u
-        if f == 0 and g == 0:
-            place = xg.at[x_rows(yy, half, u), feature_cols(xx, c)]
-        else:
-            remote(place, place, x_send, ring_recv.at[slot], partner).wait_recv()
-        first, second = (along_x, along_y) if half == 0 else (along_y, along_x)
-        for which, way, ff, gg in x_forwards(f, g, u):
-            remote(
-                place,
-                place,
-                x_send,
-                ring_recv.at[32 * half + 8 * ff + 2 * gg + u],
-                (second if which else first)[way],
-            ).start()
-        if f or g:
-            remote(others, others, xd_send, xd_recv, partner).start()
-
-    for u in range(2):
-        for half in range(2):
-            x_event(half, 0, 0, u)
+        remote(place, place, x_send, ring_recv.at[slot], partner).wait_recv()
+        remote(others, others, xd_send, xd_recv, partner).start()
+
+    x_actions = x_order()
+    x_first = [action for action in x_actions if action[0][1:3] == (0, 0)]
+    for block, send in x_first[:8]:
+        x_send_on(block, send)
 
     @pl.when(c == 0)
     def _():
@@ -392,9 +419,13 @@
 
     ways = (up, down)
 
+    def z_last(way, k):
+        return 8 if (k in (0, 1, 4)) == (way == 0) else 7
+
+
     def w_on(way, d, k, origin):
         here = w_at(origin, k)
-        if d < 8 - way:
+        if d < z_last(way, k):
             remote(here, here, wz_send, ring_recv.at[4 * origin + k], ways[way]).start()
         if d == 0 and way == 0:
             return
@@ -427,10 +458,10 @@
         half = lax.div(k, 2)
         return ow.at[half, rows(y * 128 + (k - 2 * half) * 64, 64), ow_cols(x)]
 
-    def ow_on(way, d, origin):
-        here = owz.at[origin]
-        if d < 8 - way:
-            remote(here, here, oz_send, oz_recv.at[origin], ways[way]).start()
+    def ow_on(way, d, cc, origin):
+        here = owz.at[origin, cc]
+        if d < z_last(way, 4 + cc):
+            remote(here, here, oz_send, oz_recv.at[origin, cc], ways[way]).start()
 
     def ow_give(n, carry):
         turn = lax.div(n, 4)
@@ -455,15 +486,18 @@
         return carry
 
     def ow_start():
-        remote(owz.at[z, 0], owz.at[z, 0], oz_send, ox_recv, partner).wait_recv()
-        ow_on(0, 0, z)
-        ow_on(1, 0, z)
+        for cc in (1, 0):
+            if cc == 0:
+                here = owz.at[z, 0]
+                remote(here, here, oz_send, ox_recv, partner).wait_recv()
+            ow_on(0, 0, cc, z)
+            ow_on(1, 0, cc, z)
 
     def ow_event(way, d, k):
         origin = wrap(z - d if way == 0 else z + d, NZ)
-        here = owz.at[origin]
-        remote(here, here, oz_send, oz_recv.at[origin], up).wait_recv()
-        ow_on(way, d, origin)
+        here = owz.at[origin, k - 4]
+        remote(here, here, oz_send, oz_recv.at[origin, k - 4], up).wait_recv()
+        ow_on(way, d, k - 4, origin)
 
     mark("params")
     for fetch in fetches[12:]:
@@ -504,19 +538,24 @@
 
     z_agenda = []
     for way in range(2):
-        for d in range(1, 9 - way):
-            for k in range(5):
-                call = ow_event if k == 4 else w_event
+        for d in range(1, 9):
+            for k in range(6):
+                if d > z_last(way, k):
+                    continue
+                call = ow_event if k >= 4 else w_event
                 z_agenda.append((W_HOP * d + W_PART * k, call, (way, d, k)))
     z_agenda.sort(key=lambda entry: entry[0])
     mark("gather")
 
     @pl.when(c == 0)
     def _():
-        for n, (_, *event) in enumerate(x_order()):
-            if n % 15 == 0:
+        for n, (block, send) in enumerate(x_actions):
+            if n % 30 == 0:
                 mark(f"x{n}")
-            x_event(*event)
+            if send is None:
+                x_wait(block)
+            elif (block, send) not in x_first[:8]:
+                x_send_on(block, send)
         mark("w_arrive")
         everything = w.at[pl.ds(0, 2048), :]
         remote(everything, everything, wd_send, wd_recv, partner).wait_recv()
@@ -524,6 +563,8 @@
 
     @pl.when(c == 1)
     def _():
+        for block, send in x_first[8:]:
+            x_send_on(block, send)
         for k in range(4):
             w_start(k)
         ow_start()
@@ -1023,7 +1064,7 @@
             dma,
             dma,
             dma,
-            dma((NZ,)),
+            dma((NZ, 2)),
             dma,
             dma((4,)),
             dma,

time: 74.9 us -> 74.4 us (level)
  no operation moved by 1% of the time
where the time goes in v5:
time: 74.4 us; the launch traced here: 74.2 us
  Pallas kernels  72.5 us (97%)
  local copies, waits for them, and re-layouts  1.67 us (2%)
    pallas_call x1, Pallas kernels, shards(): pl.pallas_call(body, out_shape=jax.ShapeDtypeStruct((TOK, 512), BF16), in...  72.5 us
    unnamed x1, local copies, waits for them, and re-layouts  1.67 us

profile of v5, /device:TPU:1, one launch (start us, length us, event | category | flops | bytes accessed | tf_op | source)
XLA Modules:
  0.0 74.2 jit_solution(12614628192247206374)
XLA Ops:
  0.0 72.5 %mixer.1 = bf16[256,512]{1,0:T(8,128)(2,1)} custom-call(bf16[256,512]{1,0:T(8,128)(2,1)} %bitcast.14, f32[32,128]{1,0:T(8,128)} %bitcast.16, bf16[64,128]{1,0:T(8,128)(2,1)} %a_hbm.1, bf16[64,128]{1,0:T(8,128)(2,1)} %b_hbm.1, bf16[64,64]{1,0:T(8,128)(2,1)} %q_hbm.1, bf16[64,64]{1,0:T(8,128)(2,1)} %k_hbm.1, bf16[64,128]{1,0:T(8,128)(2,1)} %v_hbm.1, ...), custom_call_target="tpu_custom_call" | custom-call | tf_op jit(solution)/shard_map/mixer/pallas_call | solution.py:1012
  72.5 1.7 %copy.19 = bf16[1,256,512]{2,1,0:T(8,128)(2,1)} copy(bf16[1,256,512]{2,1,0:T(8,128)(2,1)} %bitcast.12) | data formatting | bytes 524288

commit v6 on v5

--- a/solution.py
+++ b/solution.py
@@ -909,20 +909,24 @@
             acts[:, act_cols(y_low)] = act_me[s]
 
     mark("act_pass")
+    def act_on(source, j):
+        block = acts.at[:, act_cols(j)]
+        for step in (2, 1, 3):
+            there = at(lax.rem(x + step, 4), y, z, c)
+            remote(source, block, act2_send, act2_recv, there).start()
+
+    def act_arrived(j):
+        block = acts.at[:, act_cols(j)]
+        remote(block, block, act_send, act_recv.at[j], partner).wait_recv()
+        act_on(block, j)
+
+    pl.when(y_half == c)(lambda: act_on(act_me.at[y_low], y_low))
     oy_pass(0, 0)
     oy_pass(1, 3)
     oy_pass(0, 1)
     oy_pass(1, 2)
-    for n, j in enumerate((y_low, 1 - y_low)):
-        block = acts.at[:, act_cols(j)]
-        arrived = remote(block, block, act_send, act_recv.at[j], partner)
-        if n == 0:
-            pl.when(y_half != c)(arrived.wait_recv)
-        else:
-            arrived.wait_recv()
-        for step in (2, 1, 3):
-            there = at(lax.rem(x + step, 4), y, z, c)
-            remote(block, block, act2_send, act2_recv, there).start()
+    pl.when(y_half != c)(lambda: act_arrived(y_low))
+    act_arrived(1 - y_low)
 
     mark("oy_rest")
     for ahead in (3, 2):

time: 74.4 us -> 74.4 us (level)
  no operation moved by 1% of the time
where the time goes in v6:
time: 74.4 us; the launch traced here: 74.2 us
  Pallas kernels  72.5 us (97%)
  local copies, waits for them, and re-layouts  1.67 us (2%)
    pallas_call x1, Pallas kernels, shards(): pl.pallas_call(body, out_shape=jax.ShapeDtypeStruct((TOK, 512), BF16), in...  72.5 us
    unnamed x1, local copies, waits for them, and re-layouts  1.67 us

profile of v6, /device:TPU:1, one launch (start us, length us, event | category | flops | bytes accessed | tf_op | source)
XLA Modules:
  0.0 74.2 jit_solution(4743170572692535012)
XLA Ops:
  0.0 72.5 %mixer.1 = bf16[256,512]{1,0:T(8,128)(2,1)} custom-call(bf16[256,512]{1,0:T(8,128)(2,1)} %bitcast.14, f32[32,128]{1,0:T(8,128)} %bitcast.16, bf16[64,128]{1,0:T(8,128)(2,1)} %a_hbm.1, bf16[64,128]{1,0:T(8,128)(2,1)} %b_hbm.1, bf16[64,64]{1,0:T(8,128)(2,1)} %q_hbm.1, bf16[64,64]{1,0:T(8,128)(2,1)} %k_hbm.1, bf16[64,128]{1,0:T(8,128)(2,1)} %v_hbm.1, ...), custom_call_target="tpu_custom_call" | custom-call | tf_op jit(solution)/shard_map/mixer/pallas_call | solution.py:1016
  72.5 1.7 %copy.19 = bf16[1,256,512]{2,1,0:T(8,128)(2,1)} copy(bf16[1,256,512]{2,1,0:T(8,128)(2,1)} %bitcast.12) | data formatting | bytes 524288
